TPU v7x, 512 devices: a whole 4x8x8 slice. The times are simulated.
512 devices in a mesh: fs: 64 (over z, y), tp: 8 (over x, core).
Axes of the slice: x: 4, y: 8, z: 8, core: 2. Of those that a mesh axis runs over, the one named last changes fastest.
Arguments:
- normed: bfloat16 [65536, 2048], P('fs'), may hold values from -6 to 6
- key_cot: bfloat16 [65536, 1024], P('fs', 'tp'), may hold values from -130 to 130
- value_cot: bfloat16 [65536, 2048], P('fs', 'tp'), may hold values from -130 to 130
- basis: bfloat16 [2048, 256], P('fs'), may hold values from -3.535534 to 3.535534
- master_key: float32 [2048, 1024], P('fs', 'tp'), may hold values from -3 to 3
- master_value: float32 [2048, 2048], P('fs', 'tp'), may hold values from -3 to 3
- first_key: float32 [256, 1024], P('fs', 'tp'), may hold values from -3 to 3
- second_key: float32 [256, 1024], P('fs', 'tp'), may hold values from 0.05 to 2
- first_value: float32 [256, 2048], P('fs', 'tp'), may hold values from -3 to 3
- second_value: float32 [256, 2048], P('fs', 'tp'), may hold values from 0.05 to 2
Outputs:
- step_key: float32 [2048, 1024], P('fs', 'tp')
- step_value: float32 [2048, 2048], P('fs', 'tp')
- new_master_key: float32 [2048, 1024], P('fs', 'tp')
- new_master_value: float32 [2048, 2048], P('fs', 'tp')
- copy_key: bfloat16 [2048, 1024], P(None, 'tp')
- copy_value: bfloat16 [2048, 2048], P(None, 'tp')
- new_first_key: float32 [256, 1024], P('fs', 'tp')
- new_second_key: float32 [256, 1024], P('fs', 'tp')
- new_first_value: float32 [256, 2048], P('fs', 'tp')
- new_second_value: float32 [256, 2048], P('fs', 'tp')
All inputs are finite; a program needn't handle non-finite values.
Results may differ from a plain program's by a relative error of at most 0.0055.
Values may be sent and summed in bfloat16 or wider, within the bound.
No kernel may reach another device: no remote copies, remote signals or barrier semaphores. Data moves between devices by JAX's collectives and lax.ppermute only.
A program may use at most 64 MiB of HBM per device.

v0:
```python
import jax
import jax.numpy as jnp
from jax import lax
from jax.experimental import pallas as pl
from jax.experimental.pallas import tpu as pltpu
from jax.sharding import Mesh
from jax.sharding import PartitionSpec as P

DK = 1024
DV = 2048
R = 256
FS = ("fs_0", "fs_1", "fs_2")
RING = ("fs_0", "fs_1")
TP = ("tp_0", "tp_1")

learn_rate = 0.05
beta_first = 0.9
beta_second = 0.9
epsilon = 1e-08
norm_eps = 1e-06


f32 = jnp.float32
bf16 = jnp.bfloat16
VMEM = pl.BlockSpec(memory_space=pltpu.VMEM)
SMEM = pl.BlockSpec(memory_space=pltpu.SMEM)
ANY = pl.BlockSpec(memory_space=pl.ANY)
HBM = pl.BlockSpec(memory_space=pltpu.HBM)


def shape(dims, dtype):
    return jax.ShapeDtypeStruct(dims, dtype)


def cost(flops, moved):
    return pl.CostEstimate(flops=flops, bytes_accessed=moved, transcendentals=0)


def in_hbm(array):
    return pltpu.with_memory_space_constraint(array, pltpu.HBM)


def limit(mib):
    return pltpu.CompilerParams(vmem_limit_bytes=mib * 1024 * 1024)


def dot(a, b):
    return jnp.dot(a, b, preferred_element_type=f32)


def pack_kernel(core, mk, mv, fk, fv, sk, sv, basis, pack, copies):
    kc = mk.shape[1]
    rows, half = copies.shape[1], copies.shape[2]
    pack[:rows, :kc] = mk[...].astype(bf16)
    pack[:rows, kc:] = mv[...].astype(bf16)
    keys = jnp.concatenate([fk[...], sk[...]], axis=0)
    values = jnp.concatenate([fv[...], sv[...]], axis=0)
    pack[rows:, :kc] = keys.astype(bf16)
    pack[rows:, kc:] = values.astype(bf16)
    mine = jnp.where(core[0] == 0, basis[:, :half].astype(f32), basis[:, half:].astype(f32))
    copies[...] = jnp.broadcast_to(mine.astype(bf16)[None], copies.shape)


def project_kernel(hi, lo, basis, out):
    b = basis[...]
    out[...] = (dot(hi[...], b) + dot(lo[...], b)).T


def project_both_kernel(core, hi, lo, basis, mine, out, kept, sem):
    half = mine.shape[0]
    keep = pltpu.make_async_copy(basis, kept, sem)
    keep.start()
    b = basis[...]
    at = pl.multiple_of(core[0] * half, half)
    other = pl.multiple_of((1 - core[0]) * half, half)
    out[pl.ds(at, half), :] = mine[...]
    out[pl.ds(other, half), :] = (dot(hi[...], b) + dot(lo[...], b)).T
    keep.wait()


def squares_kernel(low, out):
    x = low[...].astype(f32)
    out[...] = jnp.broadcast_to(jnp.sum(x * x, keepdims=True)[None], out.shape)


def moments(low, scale, first, second):
    scaled = low * scale
    new_first = beta_first * first + (1.0 - beta_first) * scaled
    new_second = beta_second * second + (1.0 - beta_second) * scaled * scaled
    return new_first, new_second


def pair_kernel(odd, mine, other, out):
    out[odd[0]] = mine[...]
    out[1 - odd[0]] = other[...]


def prep_kernel(gathered, first, second, mom, sem):
    n_fs, per, _ = mom.shape
    rows = gathered.shape[1] - per
    load = pltpu.make_async_copy(gathered.at[:, pl.ds(rows, per), :], mom, sem)
    load.start()
    own = per // 2
    i = lax.broadcasted_iota(jnp.int32, (n_fs * own, n_fs * per), 0)
    j = lax.broadcasted_iota(jnp.int32, (n_fs * own, n_fs * per), 1)
    at_first = (i // own) * per + i % own
    pick_first = jnp.where(j == at_first, 1.0, 0.0).astype(bf16)
    pick_second = jnp.where(j == at_first + own, 1.0, 0.0).astype(bf16)
    load.wait()
    both = mom[...].reshape(n_fs * per, mom.shape[2])
    first[...] = dot(pick_first, both).astype(bf16)
    second[...] = dot(pick_second, both).astype(bf16)


def final_kernel(
    core, squares, low_h, all_first_h, all_second_h, own_low_h, fk_h, fv_h, sk_h, sv_h, basis_h, mk_h, mv_h,
    b_mine_h, b_other_h, gathered,
    step_k, step_v, new_k, new_v, copy_k, copy_v, nf_k, ns_k, nf_v, ns_v,
    low, all_first, all_second, own_low, fk, fv, sk, sv, basis, mk, mv, b_mine, b_other,
    masters, direction, out_k, out_v,
    step_ks, step_vs, new_ks, new_vs, nf_ks, ns_ks, nf_vs, ns_vs, in_sem, master_sem, out_sem, own_sem,
):
    n_fs = masters.shape[0]
    rows = mk.shape[0]
    kc = mk.shape[1]
    half = b_mine.shape[1]
    chunks = master_sem.shape[0]
    group = n_fs // chunks
    here = (low, all_first, all_second, own_low, fk, fv, sk, sv, basis, mk, mv, b_mine, b_other)
    there = (
        low_h, all_first_h, all_second_h, own_low_h, fk_h, fv_h, sk_h, sv_h, basis_h, mk_h, mv_h,
        b_mine_h, b_other_h,
    )
    inputs = []
    for k in range(len(here)):
        inputs.append(pltpu.make_async_copy(there[k], here[k], in_sem.at[k]))
        inputs[k].start()
    loads = []
    for k in range(chunks):
        at = pl.ds(k * group, group)
        loads.append(
            pltpu.make_async_copy(
                gathered.at[at, pl.ds(0, rows), :], masters.at[at], master_sem.at[k]
            )
        )
        loads[k].start()

    stores = []

    def store(source, target, sem):
        stores.append(pltpu.make_async_copy(source, target, sem))
        stores[-1].start()

    for item in inputs[:3]:
        item.wait()
    total = jnp.sum(squares[...], axis=0)[:1, :1]
    scale = 1.0 / jnp.sqrt(total / (R * (DK + DV)) + norm_eps)

    nf, ns = moments(low[...].astype(f32), scale, all_first[...].astype(f32), all_second[...].astype(f32))
    direction[...] = (nf / (jnp.sqrt(ns) + epsilon)).astype(bf16)

    for item in inputs[3:]:
        item.wait()
    nf_ks[...], ns_ks[...] = moments(own_low[:, :kc], scale, fk[...], sk[...])
    nf_vs[...], ns_vs[...] = moments(own_low[:, kc:], scale, fv[...], sv[...])
    step = dot(basis[...], direction[...])
    step_ks[...] = step[:, :kc]
    step_vs[...] = step[:, kc:]
    new_ks[...] = mk[...] - learn_rate * step[:, :kc]
    new_vs[...] = mv[...] - learn_rate * step[:, kc:]
    sources = (step_ks, step_vs, new_ks, new_vs, nf_ks, ns_ks, nf_vs, ns_vs)
    targets = (step_k, step_v, new_k, new_v, nf_k, ns_k, nf_v, ns_v)
    for k in range(len(sources)):
        store(sources[k], targets[k], own_sem.at[k])

    at = pl.multiple_of(core[0] * half, half)
    at_other = pl.multiple_of((1 - core[0]) * half, half)
    ordered = jnp.concatenate(
        [direction[pl.ds(at, half), :], direction[pl.ds(at_other, half), :]], axis=0
    )
    for k in range(chunks):
        size = group * rows
        at = pl.ds(k * size, size)
        both = jnp.concatenate([b_mine[at, :], b_other[at, :]], axis=1)
        step = dot(both, ordered)
        loads[k].wait()
        master = masters[pl.ds(k * group, group)].astype(f32).reshape(size, -1)
        copy = (master - learn_rate * step).astype(bf16)
        out_k[at, :] = copy[:, :kc]
        out_v[at, :] = copy[:, kc:]
        store(out_k.at[at], copy_k.at[at], out_sem.at[0, k])
        store(out_v.at[at], copy_v.at[at], out_sem.at[1, k])
    for item in stores:
        item.wait()


def to_everyone(array, axis):
    copies = jnp.broadcast_to(array, (lax.axis_size(axis), *array.shape))
    return lax.all_to_all(copies, axis, split_axis=0, concat_axis=0, tiled=True)


def on_device(normed, key_cot, value_cot, basis, mk, mv, fk, sk, fv, sv):
    kc = key_cot.shape[1]
    cols = kc + value_cot.shape[1]
    rows = basis.shape[0]
    d = normed.shape[1]
    own = fk.shape[0]
    n_fs = lax.axis_size(FS)
    n_tp = lax.axis_size(TP)
    half = R // 2
    core = lax.axis_index("tp_1").astype(jnp.int32).reshape(1)
    odd = lax.axis_index("fs_2").astype(jnp.int32).reshape(1)
    per = rows + 2 * own
    pair = [(0, 1), (1, 0)]

    pack, copies = pl.pallas_call(
        pack_kernel,
        out_shape=(shape((per, cols), bf16), shape((n_fs, rows, half), bf16)),
        in_specs=[SMEM] + [VMEM] * 7,
        out_specs=(VMEM, VMEM),
        compiler_params=limit(24),
        name="pack",
    )(core, *(in_hbm(x) for x in (mk, mv, fk, fv, sk, sv, basis)))
    other_pack = lax.ppermute(pack, "fs_2", pair)
    both_packs = pl.pallas_call(
        pair_kernel,
        out_shape=shape((2, per, cols), bf16),
        in_specs=[SMEM] + [VMEM] * 2,
        out_specs=VMEM,
        compiler_params=limit(24),
        name="pair",
    )(odd, pack, other_pack)
    gathered = lax.all_gather(both_packs.reshape(2 * per, cols), RING, axis=0, tiled=True)
    gathered = gathered.reshape(n_fs, per, cols)
    basis_mine = lax.all_to_all(copies, FS, 0, 0, tiled=True).reshape(d, half)

    cot = jnp.concatenate([key_cot, value_cot], axis=1)
    grad = lax.dot_general(cot, normed, (((0,), (0,)), ((), ())), preferred_element_type=f32)
    hi = grad.astype(bf16)
    lo = (grad - hi.astype(f32)).astype(bf16)
    basis_mine, hi, lo = lax.optimization_barrier((basis_mine, hi, lo))
    basis_other = lax.ppermute(basis_mine, "tp_1", pair)
    project_cost = cost(4 * d * half * cols, 4 * d * cols + 2 * d * half)
    low_mine = pl.pallas_call(
        project_kernel,
        out_shape=shape((half, cols), f32),
        in_specs=[VMEM] * 3,
        out_specs=VMEM,
        cost_estimate=project_cost,
        compiler_params=limit(12),
        name="project_mine",
    )(hi, lo, basis_mine)
    parts, basis_other = pl.pallas_call(
        project_both_kernel,
        out_shape=(shape((R, cols), f32), pltpu.HBM((d, half), bf16)),
        in_specs=[SMEM] + [VMEM] * 4,
        out_specs=(VMEM, HBM),
        scratch_shapes=[pltpu.SemaphoreType.DMA],
        cost_estimate=project_cost,
        compiler_params=limit(12),
        name="project_other",
    )(core, hi, lo, basis_other, low_mine)
    tiles = lax.all_to_all(parts.reshape(n_fs, own, cols), FS, 0, 0, tiled=True)
    own_low = jnp.sum(tiles, axis=0)

    all_low = to_everyone(own_low.astype(bf16), FS).reshape(R, cols)
    local = pl.pallas_call(
        squares_kernel,
        out_shape=shape((n_tp, 8, 128), f32),
        in_specs=[VMEM],
        out_specs=VMEM,
        compiler_params=limit(4),
        name="squares",
    )(all_low)
    squares = lax.all_to_all(local, TP, 0, 0, tiled=True)
    all_first, all_second = pl.pallas_call(
        prep_kernel,
        out_shape=(shape((R, cols), bf16), shape((R, cols), bf16)),
        in_specs=[ANY],
        out_specs=(VMEM, VMEM),
        scratch_shapes=[
            pltpu.VMEM((n_fs, 2 * own, cols), bf16),
            pltpu.SemaphoreType.DMA,
        ],
        cost_estimate=cost(4 * R * 2 * R * cols, 2 * n_fs * per * cols),
        compiler_params=limit(24),
        name="prep",
    )(in_hbm(gathered))

    chunks = 8
    vc = cols - kc
    small = ((rows, kc), (rows, vc)) * 2 + ((own, kc), (own, kc), (own, vc), (own, vc))
    outs = tuple(shape(dims, f32) for dims in small)
    return pl.pallas_call(
        final_kernel,
        out_shape=outs[:4] + (shape((d, kc), bf16), shape((d, vc), bf16)) + outs[4:],
        in_specs=[SMEM, VMEM] + [ANY] * 14,
        out_specs=(HBM,) * 10,
        scratch_shapes=[
            pltpu.VMEM((R, cols), bf16),
            pltpu.VMEM((R, cols), bf16),
            pltpu.VMEM((R, cols), bf16),
            pltpu.VMEM((own, cols), f32),
            pltpu.VMEM((own, kc), f32),
            pltpu.VMEM((own, vc), f32),
            pltpu.VMEM((own, kc), f32),
            pltpu.VMEM((own, vc), f32),
            pltpu.VMEM((rows, R), bf16),
            pltpu.VMEM((rows, kc), f32),
            pltpu.VMEM((rows, vc), f32),
            pltpu.VMEM((d, half), bf16),
            pltpu.VMEM((d, half), bf16),
            pltpu.VMEM((n_fs, rows, cols), bf16),
            pltpu.VMEM((R, cols), bf16),
            pltpu.VMEM((d, kc), bf16),
            pltpu.VMEM((d, vc), bf16),
        ]
        + [pltpu.VMEM(dims, f32) for dims in small]
        + [
            pltpu.SemaphoreType.DMA((13,)),
            pltpu.SemaphoreType.DMA((chunks,)),
            pltpu.SemaphoreType.DMA((2, chunks)),
            pltpu.SemaphoreType.DMA((8,)),
        ],
        compiler_params=limit(40),
        name="update",
    )(
        core, squares, all_low, all_first, all_second, own_low,
        *(in_hbm(x) for x in (fk, fv, sk, sv, basis, mk, mv, basis_mine, basis_other, gathered)),
    )


def solution(mesh):
    names = ("fs_0", "fs_1", "fs_2", "tp_0", "tp_1")
    torus = Mesh(mesh.devices.reshape(8, 4, 2, 4, 2), names)
    split = P(FS, TP)
    in_specs = (P(FS, None), split, split, P(FS, None)) + (split,) * 6
    out_specs = (split,) * 4 + (P(None, TP),) * 2 + (split,) * 4
    return jax.shard_map(
        on_device, mesh=torus, in_specs=in_specs, out_specs=out_specs, check_vma=False
    )
```

profile of v0, /device:TPU:1, one launch (start us, length us, event | category | flops | bytes accessed | tf_op | source)
XLA Modules:
  0.0 125.6 jit_solution(12471364652755628698)
XLA Ops:
  7.2 0.0 all-gather.2.cloned.1.call-start
  7.2 1.7 %pack.1 = (bf16[40,384]{1,0:T(8,128)(2,1)S(1)}, bf16[64,32,128]{2,1,0:T(8,128)(2,1)}) custom-call(s32[1]{0:T(128)} %bitcast.core, f32[32,128]{1,0:T(8,128)} %mk_h.1, f32[32,256]{1,0:T(8,128)} %mv_h.1, f32[4,128]{1,0:T(4,128)} %fk_h.1, f32[4,256]{1,0:T(4,128)} %fv_h.1, f32[4,128]{1,0:T(4,128)} %sk_h.1, f32[4,256]{1,0:T(4,128)} %sv_h.1, bf16[32,256]{1,0:T(8,128)(2,1)} %basis_h.1), custom_call_target="tpu_custom_call" | custom-call | tf_op jit(solution)/shard_map/pack/pallas_call | solution.py:216
  8.9 4.0 %collective-permute-start.1 = (bf16[40,384]{1,0:T(8,128)(2,1)S(1)}, bf16[40,384]{1,0:T(8,128)(2,1)S(1)}, u32[]{:S(2)}, u32[]{:S(2)}) collective-permute-start(bf16[40,384]{1,0:T(8,128)(2,1)S(1)} %get-tuple-element.24.mine), channel_id=1, source_target_pairs={{0,8},{8,0},{1,9},{9,1},{2,10},{10,2},{3,11},{11,3},{4,12},{12,4},... | collective-permute-start | bytes 92168 | tf_op jit(solution)/shard_map/ppermute | solution.py:224
  12.9 1.3 %collective-permute-done.1.other = bf16[40,384]{1,0:T(8,128)(2,1)S(1)} collective-permute-done((bf16[40,384]{1,0:T(8,128)(2,1)S(1)}, bf16[40,384]{1,0:T(8,128)(2,1)S(1)}, u32[]{:S(2)}, u32[]{:S(2)}) %collective-permute-start.1) | collective-permute-done | bytes 30752 | tf_op jit(solution)/shard_map/ppermute | solution.py:224
  14.2 0.6 pair.1
  14.8 0.0 all-gather.2.cloned.1.call-update
  14.8 16.7 %all-to-all-start = ((bf16[64,32,128]{2,1,0:T(8,128)(2,1)}), bf16[64,32,128]{2,1,0:T(8,128)(2,1)}, u32[]{:S(2)}, u32[]{:S(2)}) async-start(bf16[64,32,128]{2,1,0:T(8,128)(2,1)} %get-tuple-element.19), calls=%async_computation | async-start | bytes 1048576 | tf_op jit(solution)/shard_map/all_to_all | solution.py:235
  31.6 4.3 %subtract_convert_fusion = (bf16[384,2048]{1,0:T(8,128)(2,1)S(1)}, bf16[384,2048]{1,0:T(8,128)(2,1)S(1)}) fusion(bf16[1024,2048]{1,0:T(8,128)(2,1)} %param.10, bf16[1024,256]{1,0:T(8,128)(2,1)} %param.12, bf16[1024,128]{1,0:T(8,128)(2,1)} %param.11), kind=kOutput, calls=%fused_computation | convolution fusion | flops 1615331328 | bytes 8126464 | tf_op jit(solution)/shard_map/dot_general | solution.py:238
  35.9 11.5 %all-to-all-done = bf16[64,32,128]{2,1,0:T(8,128)(2,1)} async-done(((bf16[64,32,128]{2,1,0:T(8,128)(2,1)}), bf16[64,32,128]{2,1,0:T(8,128)(2,1)}, u32[]{:S(2)}, u32[]{:S(2)}) %all-to-all-start) | async-done | bytes 524320 | tf_op jit(solution)/shard_map/all_to_all | solution.py:235
  47.3 7.8 %collective-permute-start = (bf16[2048,128]{1,0:T(8,128)(2,1)}, bf16[2048,128]{1,0:T(8,128)(2,1)S(1)}, u32[]{:S(2)}, u32[]{:S(2)}) collective-permute-start(bf16[2048,128]{1,0:T(8,128)(2,1)} %bitcast.1.basis.b_mine_h), channel_id=1, source_target_pairs={{0,1},{1,0},{2,3},{3,2},{4,5},{5,4},{6,7},{7,6},{8,9},{9,8},{10,11... | collective-permute-start | bytes 1572872 | tf_op jit(solution)/shard_map/ppermute | solution.py:242
  55.1 2.1 %project_mine.1.mine = f32[128,384]{1,0:T(8,128)S(1)} custom-call(bf16[384,2048]{1,0:T(8,128)(2,1)S(1)} %get-tuple-element.20.hi, bf16[384,2048]{1,0:T(8,128)(2,1)S(1)} %get-tuple-element.21.lo, bf16[2048,128]{1,0:T(8,128)(2,1)} %bitcast.1.basis.b_mine_h), custom_call_target="tpu_custom_call" | custom-call | flops 402653184 | bytes 3670016 | tf_op jit(solution)/shard_map/project_mine/pallas_call | solution.py:244
  57.2 0.0 collective-permute-done.basis
  57.2 1.1 project_other.1
  58.3 0.1 reshape.43
  58.4 20.2 %all_to_all.20 = f32[64,4,384]{2,1,0:T(4,128)S(1)} all-to-all(f32[64,4,384]{2,1,0:T(4,128)S(1)} %reshape.43), channel_id=1, replica_groups=mesh['fs_0'=8,'fs_1'=4,'fs_2'=2,'tp_0'=4,'tp_1'=2] {'fs_0','fs_1','fs_2'}, dimensions={0} | all-to-all | bytes 786432 | tf_op jit(solution)/shard_map/all_to_all | solution.py:263
  78.6 0.1 reduce_sum.9.own_low_h
  78.7 0.1 broadcast_in_dim.3
  78.8 20.9 %all_to_all.21 = bf16[64,4,384]{2,1,0:T(4,128)(2,1)S(1)} all-to-all(bf16[64,4,384]{2,1,0:T(4,128)(2,1)S(1)} %broadcast_in_dim.3), channel_id=1, replica_groups=mesh['fs_0'=8,'fs_1'=4,'fs_2'=2,'tp_0'=4,'tp_1'=2] {'fs_0','fs_1','fs_2'}, dimensions={0} | all-to-all | bytes 393216 | tf_op jit(solution)/shard_map/all_to_all | solution.py:199
  99.7 0.1 reshape.44.low.low_h
  99.7 0.8 squares.1
  100.6 7.8 %all-to-all-start.3 = ((f32[8,8,128]{2,1,0:T(8,128)}), f32[8,8,128]{2,1,0:T(8,128)S(1)}, u32[]{:S(2)}, u32[]{:S(2)}) async-start(f32[8,8,128]{2,1,0:T(8,128)} %squares.1), calls=%async_computation.3 | async-start | bytes 65536 | tf_op jit(solution)/shard_map/all_to_all | solution.py:275
  108.4 0.0 all-gather.2.cloned.1.call-done
  108.4 1.4 %prep.1 = (bf16[256,384]{1,0:T(8,128)(2,1)S(1)}, bf16[256,384]{1,0:T(8,128)(2,1)S(1)}) custom-call(bf16[64,40,384]{2,1,0:T(8,128)(2,1)} %bitcast.6), custom_call_target="tpu_custom_call" | custom-call | flops 201326592 | bytes 1966080 | tf_op jit(solution)/shard_map/prep/pallas_call | solution.py:276
  109.8 3.3 %all-to-all-done.3.squares = f32[8,8,128]{2,1,0:T(8,128)S(1)} async-done(((f32[8,8,128]{2,1,0:T(8,128)}), f32[8,8,128]{2,1,0:T(8,128)S(1)}, u32[]{:S(2)}, u32[]{:S(2)}) %all-to-all-start.3) | async-done | bytes 32800 | tf_op jit(solution)/shard_map/all_to_all | solution.py:275
  113.1 5.7 %update.1 = (f32[32,128]{1,0:T(8,128)}, f32[32,256]{1,0:T(8,128)}, f32[32,128]{1,0:T(8,128)}, f32[32,256]{1,0:T(8,128)}, bf16[2048,128]{1,0:T(8,128)(2,1)}, /*in...) custom-call(s32[1]{0:T(128)} %bitcast.core, ...), custom_call_target="tpu_custom_call" | custom-call | tf_op jit(solution)/shard_map/update/pallas_call | solution.py:294
  (1 shorter events, 0.0 us)
Async XLA Ops:
  7.2 101.2 %all-gather.2.cloned.1.call-start = ((), (), s32[]{:S(2)}) async-start(), calls=%async_computation.4 | async-start | bytes 2027520 | tf_op jit(solution)/shard_map/all_gather | solution.py:233
  8.9 5.3 %collective-permute-start.1 = (bf16[40,384]{1,0:T(8,128)(2,1)S(1)}, bf16[40,384]{1,0:T(8,128)(2,1)S(1)}, u32[]{:S(2)}, u32[]{:S(2)}) collective-permute-start(bf16[40,384]{1,0:T(8,128)(2,1)S(1)} %get-tuple-element.24.mine), channel_id=1, source_target_pairs={{0,8},{8,0},{1,9},{9,1},{2,10},{10,2},{3,11},{11,3},{4,12},{12,4},... | collective-permute-start | bytes 92168 | tf_op jit(solution)/shard_map/ppermute | solution.py:224
  14.8 32.5 %all-to-all-start = ((bf16[64,32,128]{2,1,0:T(8,128)(2,1)}), bf16[64,32,128]{2,1,0:T(8,128)(2,1)}, u32[]{:S(2)}, u32[]{:S(2)}) async-start(bf16[64,32,128]{2,1,0:T(8,128)(2,1)} %get-tuple-element.19), calls=%async_computation | async-start | bytes 1048576 | tf_op jit(solution)/shard_map/all_to_all | solution.py:235
  47.3 9.9 %collective-permute-start = (bf16[2048,128]{1,0:T(8,128)(2,1)}, bf16[2048,128]{1,0:T(8,128)(2,1)S(1)}, u32[]{:S(2)}, u32[]{:S(2)}) collective-permute-start(bf16[2048,128]{1,0:T(8,128)(2,1)} %bitcast.1.basis.b_mine_h), channel_id=1, source_target_pairs={{0,1},{1,0},{2,3},{3,2},{4,5},{5,4},{6,7},{7,6},{8,9},{9,8},{10,11... | collective-permute-start | bytes 1572872 | tf_op jit(solution)/shard_map/ppermute | solution.py:242
  100.6 12.5 %all-to-all-start.3 = ((f32[8,8,128]{2,1,0:T(8,128)}), f32[8,8,128]{2,1,0:T(8,128)S(1)}, u32[]{:S(2)}, u32[]{:S(2)}) async-start(f32[8,8,128]{2,1,0:T(8,128)} %squares.1), calls=%async_computation.3 | async-start | bytes 65536 | tf_op jit(solution)/shard_map/all_to_all | solution.py:275
Sparse Core Ops, SparseCore 0:
  14.9 91.2 all-gather.1
where the time goes:
time: 126 us
  blocking collectives  41.1 us (33%)
  starting transfers between devices  36.4 us (29%)
  waiting for transfers between devices  16 us (13%)
  between operations  14.1 us (11%)
  Pallas kernels  13.4 us (11%)
  matrix products  4.28 us (3%)
    all_to_all x1, blocking collectives, to_everyone(): return lax.all_to_all(copies, axis, split_axis=0, concat_axis=0, tiled=True)  20.9 us
    all_to_all x1, blocking collectives, on_device(): tiles = lax.all_to_all(parts.reshape(n_fs, own, cols), FS, 0, 0, tiled=True)  20.2 us
    all_to_all x1, starting transfers between devices, on_device(): basis_mine = lax.all_to_all(copies, FS, 0, 0, tiled=True).reshape(d, half)  16.7 us
    all_to_all x1, waiting for transfers between devices, on_device(): basis_mine = lax.all_to_all(copies, FS, 0, 0, tiled=True).reshape(d, half)  11.5 us
    all_to_all x1, starting transfers between devices, on_device(): squares = lax.all_to_all(local, TP, 0, 0, tiled=True)  7.81 us
    ppermute x1, starting transfers between devices, on_device(): basis_other = lax.ppermute(basis_mine, 'tp_1', pair)  7.8 us
    pallas_call x1, Pallas kernels, on_device(): pl.pallas_call(final_kernel, out_shape=outs[:4] + (shape((d, kc), bf16),...  5.67 us
    dot_general x1, matrix products, on_device(): lax.dot_general(cot, normed, (((0,), (0,)), ((), ())), preferred_element_...  4.28 us
  transfers between devices with their start and end apart: 5, of which 3 were waited for; matrix products, arithmetic and copies ran while one was open for 4% of the time, Pallas kernels for 4%

commit v1 on v0

--- a/solution.py
+++ b/solution.py
@@ -9,8 +9,9 @@
 DK = 1024
 DV = 2048
 R = 256
-FS = ("fs_0", "fs_1", "fs_2")
-RING = ("fs_0", "fs_1")
+FS = ("fs_0", "fs_1", "fs_2", "fs_3")
+RING = ("fs_0",)
+PAIRS = ("fs_3", "fs_2", "fs_1")
 TP = ("tp_0", "tp_1")
 
 learn_rate = 0.05
@@ -209,7 +210,6 @@
     n_tp = lax.axis_size(TP)
     half = R // 2
     core = lax.axis_index("tp_1").astype(jnp.int32).reshape(1)
-    odd = lax.axis_index("fs_2").astype(jnp.int32).reshape(1)
     per = rows + 2 * own
     pair = [(0, 1), (1, 0)]
 
@@ -221,17 +221,19 @@
         compiler_params=limit(24),
         name="pack",
     )(core, *(in_hbm(x) for x in (mk, mv, fk, fv, sk, sv, basis)))
-    other_pack = lax.ppermute(pack, "fs_2", pair)
-    both_packs = pl.pallas_call(
-        pair_kernel,
-        out_shape=shape((2, per, cols), bf16),
-        in_specs=[SMEM] + [VMEM] * 2,
-        out_specs=VMEM,
-        compiler_params=limit(24),
-        name="pair",
-    )(odd, pack, other_pack)
-    gathered = lax.all_gather(both_packs.reshape(2 * per, cols), RING, axis=0, tiled=True)
-    gathered = gathered.reshape(n_fs, per, cols)
+    block = pack
+    for axis in PAIRS:
+        other_block = lax.ppermute(block, axis, pair)
+        block = pl.pallas_call(
+            pair_kernel,
+            out_shape=shape((2, *block.shape), bf16),
+            in_specs=[SMEM] + [VMEM] * 2,
+            out_specs=VMEM,
+            compiler_params=limit(24),
+            name="pair",
+        )(lax.axis_index(axis).astype(jnp.int32).reshape(1), block, other_block)
+        block = block.reshape(-1, cols)
+    gathered = lax.all_gather(block, RING, axis=0, tiled=True).reshape(n_fs, per, cols)
     basis_mine = lax.all_to_all(copies, FS, 0, 0, tiled=True).reshape(d, half)
 
     cot = jnp.concatenate([key_cot, value_cot], axis=1)
@@ -331,8 +333,8 @@
 
 
 def solution(mesh):
-    names = ("fs_0", "fs_1", "fs_2", "tp_0", "tp_1")
-    torus = Mesh(mesh.devices.reshape(8, 4, 2, 4, 2), names)
+    names = (*FS, *TP)
+    torus = Mesh(mesh.devices.reshape(8, 2, 2, 2, 4, 2), names)
     split = P(FS, TP)
     in_specs = (P(FS, None), split, split, P(FS, None)) + (split,) * 6
     out_specs = (split,) * 4 + (P(None, TP),) * 2 + (split,) * 4

time: 126 us -> 140 us (1.11)
  starting transfers between devices: 36.4 us -> 48.3 us
  waiting for transfers between devices: 16 us -> 19 us
    ppermute x1 -> x3, starting transfers between devices: 4.01 us -> 16.5 us  [on_device(): other_block = lax.ppermute(block, axis, pair)]
    ppermute x1 -> x3, waiting for transfers between devices: 1.26 us -> 5.2 us  [on_device(): other_block = lax.ppermute(block, axis, pair)]
    all_to_all x1, blocking collectives: 20.9 us -> 18.5 us  [to_everyone(): return lax.all_to_all(copies, axis, split_axis=0, concat_axis=0, tiled=True)]
  transfers between devices with their start and end apart: 5 -> 7, of which waited for: 3 -> 5; matrix products, arithmetic and copies ran while one was open for 4% -> 3% of each run, Pallas kernels for 4% -> 4%
where the time goes in v1:
time: 140 us; the launch traced here: 139 us
  starting transfers between devices  48.3 us (34%)
  blocking collectives  39.8 us (28%)
  waiting for transfers between devices  19 us (14%)
  between operations  14.2 us (10%)
  Pallas kernels  13.5 us (10%)
  matrix products  4.19 us (3%)
    all_to_all x1, blocking collectives, on_device(): tiles = lax.all_to_all(parts.reshape(n_fs, own, cols), FS, 0, 0, tiled=True)  21.3 us
    all_to_all x1, blocking collectives, to_everyone(): return lax.all_to_all(copies, axis, split_axis=0, concat_axis=0, tiled=True)  18.5 us
    all_to_all x1, starting transfers between devices, on_device(): basis_mine = lax.all_to_all(copies, FS, 0, 0, tiled=True).reshape(d, half)  17.1 us
    ppermute x3, starting transfers between devices, on_device(): other_block = lax.ppermute(block, axis, pair)  16.5 us
    all_to_all x1, waiting for transfers between devices, on_device(): basis_mine = lax.all_to_all(copies, FS, 0, 0, tiled=True).reshape(d, half)  10.5 us
    ppermute x1, starting transfers between devices, on_device(): basis_other = lax.ppermute(basis_mine, 'tp_1', pair)  7.71 us
    all_to_all x1, starting transfers between devices, on_device(): squares = lax.all_to_all(local, TP, 0, 0, tiled=True)  6.96 us
    pallas_call x1, Pallas kernels, on_device(): pl.pallas_call(final_kernel, out_shape=outs[:4] + (shape((d, kc), bf16),...  5.68 us
  transfers between devices with their start and end apart: 7, of which 5 were waited for; matrix products, arithmetic and copies ran while one was open for 3% of the time, Pallas kernels for 4%

profile of v1, /device:TPU:1, one launch (start us, length us, event | category | flops | bytes accessed | tf_op | source)
XLA Modules:
  0.0 139.3 jit_solution(11998437492556981746)
XLA Ops:
  7.2 0.0 copy-start
  7.2 0.0 all-gather.2.cloned.1.call-start
  7.2 1.7 %pack.1 = (bf16[40,384]{1,0:T(8,128)(2,1)S(1)}, bf16[64,32,128]{2,1,0:T(8,128)(2,1)}) custom-call(s32[1]{0:T(128)} %bitcast.core, f32[32,128]{1,0:T(8,128)} %mk_h.1, f32[32,256]{1,0:T(8,128)} %mv_h.1, f32[4,128]{1,0:T(4,128)} %fk_h.1, f32[4,256]{1,0:T(4,128)} %fv_h.1, f32[4,128]{1,0:T(4,128)} %sk_h.1, f32[4,256]{1,0:T(4,128)} %sv_h.1, bf16[32,256]{1,0:T(8,128)(2,1)} %basis_h.1), custom_call_target="tpu_custom_call" | custom-call | tf_op jit(solution)/shard_map/pack/pallas_call | solution.py:216
  8.9 4.0 %collective-permute-start.1 = (bf16[40,384]{1,0:T(8,128)(2,1)S(1)}, bf16[40,384]{1,0:T(8,128)(2,1)S(1)}, u32[]{:S(2)}, u32[]{:S(2)}) collective-permute-start(bf16[40,384]{1,0:T(8,128)(2,1)S(1)} %get-tuple-element.24.mine), channel_id=1, source_target_pairs={{0,8},{8,0},{1,9},{9,1},{2,10},{10,2},{3,11},{11,3},{4,12},{12,4},... | collective-permute-start | bytes 92168 | tf_op jit(solution)/shard_map/ppermute | solution.py:226
  12.9 1.3 collective-permute-done.1.other
  14.2 4.4 %collective-permute-start.2 = (bf16[80,384]{1,0:T(8,128)(2,1)S(1)}, bf16[80,384]{1,0:T(8,128)(2,1)S(1)}, u32[]{:S(2)}, u32[]{:S(2)}) collective-permute-start(bf16[80,384]{1,0:T(8,128)(2,1)S(1)} %bitcast.12), channel_id=1, source_target_pairs={{0,16},{16,0},{1,17},{17,1},{2,18},{18,2},{3,19},{19,3},{4,20},{20... | collective-permute-start | bytes 184328 | tf_op jit(solution)/shard_map/ppermute | solution.py:226
  18.6 1.6 %collective-permute-done.2.other = bf16[80,384]{1,0:T(8,128)(2,1)S(1)} collective-permute-done((bf16[80,384]{1,0:T(8,128)(2,1)S(1)}, bf16[80,384]{1,0:T(8,128)(2,1)S(1)}, u32[]{:S(2)}, u32[]{:S(2)}) %collective-permute-start.2) | collective-permute-done | bytes 61472 | tf_op jit(solution)/shard_map/ppermute | solution.py:226
  20.2 8.2 %collective-permute-start.3 = (bf16[160,384]{1,0:T(8,128)(2,1)S(1)}, bf16[160,384]{1,0:T(8,128)(2,1)S(1)}, u32[]{:S(2)}, u32[]{:S(2)}) collective-permute-start(bf16[160,384]{1,0:T(8,128)(2,1)S(1)} %bitcast.10), channel_id=1, source_target_pairs={{0,32},{32,0},{1,33},{33,1},{2,34},{34,2},{3,35},{35,3},{4,36},{36... | collective-permute-start | bytes 368648 | tf_op jit(solution)/shard_map/ppermute | solution.py:226
  28.4 2.3 %collective-permute-done.3.other = bf16[160,384]{1,0:T(8,128)(2,1)S(1)} collective-permute-done((bf16[160,384]{1,0:T(8,128)(2,1)S(1)}, bf16[160,384]{1,0:T(8,128)(2,1)S(1)}, u32[]{:S(2)}, u32[]{:S(2)}) %collective-permute-start.3) | collective-permute-done | bytes 122912 | tf_op jit(solution)/shard_map/ppermute | solution.py:226
  30.7 0.7 pair.5
  31.4 0.0 all-gather.2.cloned.1.call-update
  31.5 17.1 %all-to-all-start = ((bf16[64,32,128]{2,1,0:T(8,128)(2,1)}), bf16[64,32,128]{2,1,0:T(8,128)(2,1)}, u32[]{:S(2)}, u32[]{:S(2)}) async-start(bf16[64,32,128]{2,1,0:T(8,128)(2,1)} %get-tuple-element.19), calls=%async_computation | async-start | bytes 1048576 | tf_op jit(solution)/shard_map/all_to_all | solution.py:237
  48.5 0.0 copy-done
  48.5 4.2 %subtract_convert_fusion = (bf16[384,2048]{1,0:T(8,128)(2,1)S(1)}, bf16[384,2048]{1,0:T(8,128)(2,1)S(1)}) fusion(bf16[1024,2048]{1,0:T(8,128)(2,1)} %param.10, bf16[1024,256]{1,0:T(8,128)(2,1)} %param.12, bf16[1024,128]{1,0:T(8,128)(2,1)S(1)} %copy-done), kind=kOutput, calls=%fused_computation | convolution fusion | flops 1615331328 | bytes 8126464 | tf_op jit(solution)/shard_map/dot_general | solution.py:240
  52.7 10.5 %all-to-all-done = bf16[64,32,128]{2,1,0:T(8,128)(2,1)} async-done(((bf16[64,32,128]{2,1,0:T(8,128)(2,1)}), bf16[64,32,128]{2,1,0:T(8,128)(2,1)}, u32[]{:S(2)}, u32[]{:S(2)}) %all-to-all-start) | async-done | bytes 524320 | tf_op jit(solution)/shard_map/all_to_all | solution.py:237
  63.2 7.7 %collective-permute-start = (bf16[2048,128]{1,0:T(8,128)(2,1)}, bf16[2048,128]{1,0:T(8,128)(2,1)S(1)}, u32[]{:S(2)}, u32[]{:S(2)}) collective-permute-start(bf16[2048,128]{1,0:T(8,128)(2,1)} %bitcast.1.basis.b_mine_h), channel_id=1, source_target_pairs={{0,1},{1,0},{2,3},{3,2},{4,5},{5,4},{6,7},{7,6},{8,9},{9,8},{10,11... | collective-permute-start | bytes 1572872 | tf_op jit(solution)/shard_map/ppermute | solution.py:244
  70.9 2.1 %project_mine.1.mine = f32[128,384]{1,0:T(8,128)S(1)} custom-call(bf16[384,2048]{1,0:T(8,128)(2,1)S(1)} %get-tuple-element.20.hi, bf16[384,2048]{1,0:T(8,128)(2,1)S(1)} %get-tuple-element.21.lo, bf16[2048,128]{1,0:T(8,128)(2,1)} %bitcast.1.basis.b_mine_h), custom_call_target="tpu_custom_call" | custom-call | flops 402653184 | bytes 3670016 | tf_op jit(solution)/shard_map/project_mine/pallas_call | solution.py:246
  73.0 0.0 collective-permute-done.basis
  73.0 1.1 project_other.1
  74.1 0.1 reshape.55
  74.2 21.3 %all_to_all.20 = f32[64,4,384]{2,1,0:T(4,128)S(1)} all-to-all(f32[64,4,384]{2,1,0:T(4,128)S(1)} %reshape.55), channel_id=1, replica_groups=mesh['fs_0'=8,'fs_1'=2,'fs_2'=2,'fs_3'=2,'tp_0'=4,'tp_1'=2] {'fs_0','fs_..., dimensions={0} | all-to-all | bytes 786432 | tf_op jit(solution)/shard_map/all_to_all | solution.py:265
  95.5 0.1 reduce_sum.9.own_low_h
  95.6 0.1 broadcast_in_dim.3
  95.6 18.5 %all_to_all.21 = bf16[64,4,384]{2,1,0:T(4,128)(2,1)S(1)} all-to-all(bf16[64,4,384]{2,1,0:T(4,128)(2,1)S(1)} %broadcast_in_dim.3), channel_id=1, replica_groups=mesh['fs_0'=8,'fs_1'=2,'fs_2'=2,'fs_3'=2,'tp_0'=4,'tp_1'=2] {'fs_0','fs_..., dimensions={0} | all-to-all | bytes 393216 | tf_op jit(solution)/shard_map/all_to_all | solution.py:200
  114.2 0.1 reshape.56.low.low_h
  114.2 0.8 squares.1
  115.0 7.0 %all-to-all-start.3 = ((f32[8,8,128]{2,1,0:T(8,128)}), f32[8,8,128]{2,1,0:T(8,128)S(1)}, u32[]{:S(2)}, u32[]{:S(2)}) async-start(f32[8,8,128]{2,1,0:T(8,128)} %squares.1), calls=%async_computation.3 | async-start | bytes 65536 | tf_op jit(solution)/shard_map/all_to_all | solution.py:277
  122.0 0.0 all-gather.2.cloned.1.call-done
  122.0 1.4 %prep.1 = (bf16[256,384]{1,0:T(8,128)(2,1)S(1)}, bf16[256,384]{1,0:T(8,128)(2,1)S(1)}) custom-call(bf16[64,40,384]{2,1,0:T(8,128)(2,1)} %bitcast.14), custom_call_target="tpu_custom_call" | custom-call | flops 201326592 | bytes 1966080 | tf_op jit(solution)/shard_map/prep/pallas_call | solution.py:278
  123.5 3.3 %all-to-all-done.3.squares = f32[8,8,128]{2,1,0:T(8,128)S(1)} async-done(((f32[8,8,128]{2,1,0:T(8,128)}), f32[8,8,128]{2,1,0:T(8,128)S(1)}, u32[]{:S(2)}, u32[]{:S(2)}) %all-to-all-start.3) | async-done | bytes 32800 | tf_op jit(solution)/shard_map/all_to_all | solution.py:277
  126.7 5.7 %update.1 = (f32[32,128]{1,0:T(8,128)}, f32[32,256]{1,0:T(8,128)}, f32[32,128]{1,0:T(8,128)}, f32[32,256]{1,0:T(8,128)}, bf16[2048,128]{1,0:T(8,128)(2,1)}, /*in...) custom-call(s32[1]{0:T(128)} %bitcast.core, ...), custom_call_target="tpu_custom_call" | custom-call | tf_op jit(solution)/shard_map/update/pallas_call | solution.py:296
  (3 shorter events, 0.0 us)
Async XLA Ops:
  7.2 41.4 %copy-start = (bf16[1024,128]{1,0:T(8,128)(2,1)S(1)}, bf16[1024,128]{1,0:T(8,128)(2,1)}, u32[]{:S(2)}) copy-start(bf16[1024,128]{1,0:T(8,128)(2,1)} %param.11) | copy-start | bytes 786436
  7.2 114.8 %all-gather.2.cloned.1.call-start = ((), (), s32[]{:S(2)}) async-start(), calls=%async_computation.4 | async-start | bytes 2211840 | tf_op jit(solution)/shard_map/all_gather | solution.py:236
  8.9 5.3 %collective-permute-start.1 = (bf16[40,384]{1,0:T(8,128)(2,1)S(1)}, bf16[40,384]{1,0:T(8,128)(2,1)S(1)}, u32[]{:S(2)}, u32[]{:S(2)}) collective-permute-start(bf16[40,384]{1,0:T(8,128)(2,1)S(1)} %get-tuple-element.24.mine), channel_id=1, source_target_pairs={{0,8},{8,0},{1,9},{9,1},{2,10},{10,2},{3,11},{11,3},{4,12},{12,4},... | collective-permute-start | bytes 92168 | tf_op jit(solution)/shard_map/ppermute | solution.py:226
  14.2 6.0 %collective-permute-start.2 = (bf16[80,384]{1,0:T(8,128)(2,1)S(1)}, bf16[80,384]{1,0:T(8,128)(2,1)S(1)}, u32[]{:S(2)}, u32[]{:S(2)}) collective-permute-start(bf16[80,384]{1,0:T(8,128)(2,1)S(1)} %bitcast.12), channel_id=1, source_target_pairs={{0,16},{16,0},{1,17},{17,1},{2,18},{18,2},{3,19},{19,3},{4,20},{20... | collective-permute-start | bytes 184328 | tf_op jit(solution)/shard_map/ppermute | solution.py:226
  20.2 10.5 %collective-permute-start.3 = (bf16[160,384]{1,0:T(8,128)(2,1)S(1)}, bf16[160,384]{1,0:T(8,128)(2,1)S(1)}, u32[]{:S(2)}, u32[]{:S(2)}) collective-permute-start(bf16[160,384]{1,0:T(8,128)(2,1)S(1)} %bitcast.10), channel_id=1, source_target_pairs={{0,32},{32,0},{1,33},{33,1},{2,34},{34,2},{3,35},{35,3},{4,36},{36... | collective-permute-start | bytes 368648 | tf_op jit(solution)/shard_map/ppermute | solution.py:226
  31.5 31.7 %all-to-all-start = ((bf16[64,32,128]{2,1,0:T(8,128)(2,1)}), bf16[64,32,128]{2,1,0:T(8,128)(2,1)}, u32[]{:S(2)}, u32[]{:S(2)}) async-start(bf16[64,32,128]{2,1,0:T(8,128)(2,1)} %get-tuple-element.19), calls=%async_computation | async-start | bytes 1048576 | tf_op jit(solution)/shard_map/all_to_all | solution.py:237
  63.2 9.8 %collective-permute-start = (bf16[2048,128]{1,0:T(8,128)(2,1)}, bf16[2048,128]{1,0:T(8,128)(2,1)S(1)}, u32[]{:S(2)}, u32[]{:S(2)}) collective-permute-start(bf16[2048,128]{1,0:T(8,128)(2,1)} %bitcast.1.basis.b_mine_h), channel_id=1, source_target_pairs={{0,1},{1,0},{2,3},{3,2},{4,5},{5,4},{6,7},{7,6},{8,9},{9,8},{10,11... | collective-permute-start | bytes 1572872 | tf_op jit(solution)/shard_map/ppermute | solution.py:244
  115.0 11.7 %all-to-all-start.3 = ((f32[8,8,128]{2,1,0:T(8,128)}), f32[8,8,128]{2,1,0:T(8,128)S(1)}, u32[]{:S(2)}, u32[]{:S(2)}) async-start(f32[8,8,128]{2,1,0:T(8,128)} %squares.1), calls=%async_computation.3 | async-start | bytes 65536 | tf_op jit(solution)/shard_map/all_to_all | solution.py:277
Sparse Core Ops, SparseCore 0:
  31.6 62.3 all-gather.1

commit v2 on v1

--- a/solution.py
+++ b/solution.py
@@ -10,8 +10,8 @@
 DV = 2048
 R = 256
 FS = ("fs_0", "fs_1", "fs_2", "fs_3")
-RING = ("fs_0",)
-PAIRS = ("fs_3", "fs_2", "fs_1")
+RING = ("fs_0", "fs_2")
+NEAR = ("fs_1", "fs_3")
 TP = ("tp_0", "tp_1")
 
 learn_rate = 0.05
@@ -49,15 +49,16 @@
     return jnp.dot(a, b, preferred_element_type=f32)
 
 
-def pack_kernel(core, mk, mv, fk, fv, sk, sv, basis, pack, copies):
+def pack_kernel(core, mk, mv, fk, fv, sk, sv, basis, packs, copies):
     kc = mk.shape[1]
     rows, half = copies.shape[1], copies.shape[2]
-    pack[:rows, :kc] = mk[...].astype(bf16)
-    pack[:rows, kc:] = mv[...].astype(bf16)
-    keys = jnp.concatenate([fk[...], sk[...]], axis=0)
-    values = jnp.concatenate([fv[...], sv[...]], axis=0)
-    pack[rows:, :kc] = keys.astype(bf16)
-    pack[rows:, kc:] = values.astype(bf16)
+    keys = jnp.concatenate([fk[...], sk[...]], axis=0).astype(bf16)
+    values = jnp.concatenate([fv[...], sv[...]], axis=0).astype(bf16)
+    for k in range(packs.shape[0]):
+        packs[k, :rows, :kc] = mk[...].astype(bf16)
+        packs[k, :rows, kc:] = mv[...].astype(bf16)
+        packs[k, rows:, :kc] = keys
+        packs[k, rows:, kc:] = values
     mine = jnp.where(core[0] == 0, basis[:, :half].astype(f32), basis[:, half:].astype(f32))
     copies[...] = jnp.broadcast_to(mine.astype(bf16)[None], copies.shape)
 
@@ -74,8 +75,8 @@
     b = basis[...]
     at = pl.multiple_of(core[0] * half, half)
     other = pl.multiple_of((1 - core[0]) * half, half)
-    out[pl.ds(at, half), :] = mine[...]
-    out[pl.ds(other, half), :] = (dot(hi[...], b) + dot(lo[...], b)).T
+    out[pl.ds(at, half), :] = mine[...].astype(bf16)
+    out[pl.ds(other, half), :] = (dot(hi[...], b) + dot(lo[...], b)).T.astype(bf16)
     keep.wait()
 
 
@@ -91,24 +92,28 @@
     return new_first, new_second
 
 
-def pair_kernel(odd, mine, other, out):
-    out[odd[0]] = mine[...]
-    out[1 - odd[0]] = other[...]
-
-
-def prep_kernel(gathered, first, second, mom, sem):
-    n_fs, per, _ = mom.shape
-    rows = gathered.shape[1] - per
-    load = pltpu.make_async_copy(gathered.at[:, pl.ds(rows, per), :], mom, sem)
-    load.start()
+def row_loads(gathered, start, size, target, sems):
+    zs, _, near, _, _, _ = gathered.shape
+    for z in range(zs * near):
+        source = gathered.at[z // near, :, z % near, :, pl.ds(start, size), :]
+        yield pltpu.make_async_copy(source, target.at[z], sems.at[z])
+
+
+def prep_kernel(gathered, first, second, mom, sems):
+    per, cols = mom.shape[-2:]
     own = per // 2
-    i = lax.broadcasted_iota(jnp.int32, (n_fs * own, n_fs * per), 0)
-    j = lax.broadcasted_iota(jnp.int32, (n_fs * own, n_fs * per), 1)
+    loads = list(row_loads(gathered, gathered.shape[4] - per, per, mom, sems))
+    for load in loads:
+        load.start()
+    kept = first.shape[0]
+    i = lax.broadcasted_iota(jnp.int32, (kept, 2 * kept), 0)
+    j = lax.broadcasted_iota(jnp.int32, (kept, 2 * kept), 1)
     at_first = (i // own) * per + i % own
     pick_first = jnp.where(j == at_first, 1.0, 0.0).astype(bf16)
     pick_second = jnp.where(j == at_first + own, 1.0, 0.0).astype(bf16)
-    load.wait()
-    both = mom[...].reshape(n_fs * per, mom.shape[2])
+    for load in loads:
+        load.wait()
+    both = mom[...].reshape(2 * kept, cols)
     first[...] = dot(pick_first, both).astype(bf16)
     second[...] = dot(pick_second, both).astype(bf16)
 
@@ -121,12 +126,11 @@
     masters, direction, out_k, out_v,
     step_ks, step_vs, new_ks, new_vs, nf_ks, ns_ks, nf_vs, ns_vs, in_sem, master_sem, out_sem, own_sem,
 ):
-    n_fs = masters.shape[0]
     rows = mk.shape[0]
     kc = mk.shape[1]
     half = b_mine.shape[1]
-    chunks = master_sem.shape[0]
-    group = n_fs // chunks
+    chunks = masters.shape[0]
+    size = copy_k.shape[0] // chunks
     here = (low, all_first, all_second, own_low, fk, fv, sk, sv, basis, mk, mv, b_mine, b_other)
     there = (
         low_h, all_first_h, all_second_h, own_low_h, fk_h, fv_h, sk_h, sv_h, basis_h, mk_h, mv_h,
@@ -136,15 +140,9 @@
     for k in range(len(here)):
         inputs.append(pltpu.make_async_copy(there[k], here[k], in_sem.at[k]))
         inputs[k].start()
-    loads = []
-    for k in range(chunks):
-        at = pl.ds(k * group, group)
-        loads.append(
-            pltpu.make_async_copy(
-                gathered.at[at, pl.ds(0, rows), :], masters.at[at], master_sem.at[k]
-            )
-        )
-        loads[k].start()
+    loads = list(row_loads(gathered, 0, rows, masters, master_sem))
+    for load in loads:
+        load.start()
 
     stores = []
 
@@ -180,12 +178,11 @@
         [direction[pl.ds(at, half), :], direction[pl.ds(at_other, half), :]], axis=0
     )
     for k in range(chunks):
-        size = group * rows
         at = pl.ds(k * size, size)
         both = jnp.concatenate([b_mine[at, :], b_other[at, :]], axis=1)
         step = dot(both, ordered)
         loads[k].wait()
-        master = masters[pl.ds(k * group, group)].astype(f32).reshape(size, -1)
+        master = masters[k].astype(f32).reshape(size, -1)
         copy = (master - learn_rate * step).astype(bf16)
         out_k[at, :] = copy[:, :kc]
         out_v[at, :] = copy[:, kc:]
@@ -213,27 +210,21 @@
     per = rows + 2 * own
     pair = [(0, 1), (1, 0)]
 
-    pack, copies = pl.pallas_call(
+    near = lax.axis_size(NEAR)
+    packs, copies = pl.pallas_call(
         pack_kernel,
-        out_shape=(shape((per, cols), bf16), shape((n_fs, rows, half), bf16)),
+        out_shape=(shape((near, per, cols), bf16), shape((n_fs, rows, half), bf16)),
         in_specs=[SMEM] + [VMEM] * 7,
         out_specs=(VMEM, VMEM),
         compiler_params=limit(24),
         name="pack",
     )(core, *(in_hbm(x) for x in (mk, mv, fk, fv, sk, sv, basis)))
-    block = pack
-    for axis in PAIRS:
-        other_block = lax.ppermute(block, axis, pair)
-        block = pl.pallas_call(
-            pair_kernel,
-            out_shape=shape((2, *block.shape), bf16),
-            in_specs=[SMEM] + [VMEM] * 2,
-            out_specs=VMEM,
-            compiler_params=limit(24),
-            name="pair",
-        )(lax.axis_index(axis).astype(jnp.int32).reshape(1), block, other_block)
-        block = block.reshape(-1, cols)
-    gathered = lax.all_gather(block, RING, axis=0, tiled=True).reshape(n_fs, per, cols)
+    block = lax.all_to_all(packs, NEAR, 0, 0, tiled=True).reshape(near * per, cols)
+    gathered = lax.all_gather(block, RING, axis=0, tiled=True)
+    zs, ys = lax.axis_size("fs_0"), lax.axis_size("fs_2")
+    z_near, y_near = lax.axis_size("fs_1"), lax.axis_size("fs_3")
+    gathered = gathered.reshape(zs, ys, z_near, y_near, per, cols)
+    chunks = zs * z_near
     basis_mine = lax.all_to_all(copies, FS, 0, 0, tiled=True).reshape(d, half)
 
     cot = jnp.concatenate([key_cot, value_cot], axis=1)
@@ -254,7 +245,7 @@
     )(hi, lo, basis_mine)
     parts, basis_other = pl.pallas_call(
         project_both_kernel,
-        out_shape=(shape((R, cols), f32), pltpu.HBM((d, half), bf16)),
+        out_shape=(shape((R, cols), bf16), pltpu.HBM((d, half), bf16)),
         in_specs=[SMEM] + [VMEM] * 4,
         out_specs=(VMEM, HBM),
         scratch_shapes=[pltpu.SemaphoreType.DMA],
@@ -263,7 +254,7 @@
         name="project_other",
     )(core, hi, lo, basis_other, low_mine)
     tiles = lax.all_to_all(parts.reshape(n_fs, own, cols), FS, 0, 0, tiled=True)
-    own_low = jnp.sum(tiles, axis=0)
+    own_low = jnp.sum(tiles.astype(f32), axis=0)
 
     all_low = to_everyone(own_low.astype(bf16), FS).reshape(R, cols)
     local = pl.pallas_call(
@@ -281,15 +272,14 @@
         in_specs=[ANY],
         out_specs=(VMEM, VMEM),
         scratch_shapes=[
-            pltpu.VMEM((n_fs, 2 * own, cols), bf16),
-            pltpu.SemaphoreType.DMA,
+            pltpu.VMEM((chunks, ys, y_near, 2 * own, cols), bf16),
+            pltpu.SemaphoreType.DMA((chunks,)),
         ],
         cost_estimate=cost(4 * R * 2 * R * cols, 2 * n_fs * per * cols),
         compiler_params=limit(24),
         name="prep",
     )(in_hbm(gathered))
 
-    chunks = 8
     vc = cols - kc
     small = ((rows, kc), (rows, vc)) * 2 + ((own, kc), (own, kc), (own, vc), (own, vc))
     outs = tuple(shape(dims, f32) for dims in small)
@@ -312,7 +302,7 @@
             pltpu.VMEM((rows, vc), f32),
             pltpu.VMEM((d, half), bf16),
             pltpu.VMEM((d, half), bf16),
-            pltpu.VMEM((n_fs, rows, cols), bf16),
+            pltpu.VMEM((chunks, ys, y_near, rows, cols), bf16),
             pltpu.VMEM((R, cols), bf16),
             pltpu.VMEM((d, kc), bf16),
             pltpu.VMEM((d, vc), bf16),
@@ -334,7 +324,7 @@
 
 def solution(mesh):
     names = (*FS, *TP)
-    torus = Mesh(mesh.devices.reshape(8, 2, 2, 2, 4, 2), names)
+    torus = Mesh(mesh.devices.reshape(4, 2, 4, 2, 4, 2), names)
     split = P(FS, TP)
     in_specs = (P(FS, None), split, split, P(FS, None)) + (split,) * 6
     out_specs = (split,) * 4 + (P(None, TP),) * 2 + (split,) * 4

time: 140 us -> 124 us (0.89)
  starting transfers between devices: 48.3 us -> 30.9 us
  blocking collectives: 39.8 us -> 46.1 us
  waiting for transfers between devices: 19 us -> 15.2 us
    ppermute x3 -> x0, starting transfers between devices: 16.5 us -> none  [on_device(): other_block = lax.ppermute(block, axis, pair)]
    all_to_all x0 -> x1, blocking collectives: none -> 8.93 us  [on_device(): lax.all_to_all(packs, NEAR, 0, 0, tiled=True).reshape(near * per, cols)]
    ppermute x3 -> x0, waiting for transfers between devices: 5.2 us -> none  [on_device(): other_block = lax.ppermute(block, axis, pair)]
    all_to_all x1, blocking collectives: 21.3 us -> 17.6 us  [on_device(): tiles = lax.all_to_all(parts.reshape(n_fs, own, cols), FS, 0, 0, tiled=True)]
    all_to_all x1, starting transfers between devices: 17.1 us -> 15.3 us  [on_device(): basis_mine = lax.all_to_all(copies, FS, 0, 0, tiled=True).reshape(d, half)]
    all_to_all x1, waiting for transfers between devices: 10.5 us -> 11.9 us  [on_device(): basis_mine = lax.all_to_all(copies, FS, 0, 0, tiled=True).reshape(d, half)]
    pallas_call x5 -> x2, Pallas kernels: 3.48 us -> 2.72 us  [the longest x1 1.66 us: on_device(): pl.pallas_call(pack_kernel, out_shape=(shape((near, per, cols), bf16), sh...]
  transfers between devices with their start and end apart: 7 -> 4, of which waited for: 5 -> 2; matrix products, arithmetic and copies ran while one was open for 3% -> 4% of each run, Pallas kernels for 4% -> 4%
where the time goes in v2:
time: 124 us; the launch traced here: 123 us
  blocking collectives  46.1 us (37%)
  starting transfers between devices  30.9 us (25%)
  waiting for transfers between devices  15.2 us (12%)
  between operations  14.1 us (11%)
  Pallas kernels  12.3 us (10%)
  matrix products  4.28 us (3%)
    all_to_all x1, blocking collectives, to_everyone(): return lax.all_to_all(copies, axis, split_axis=0, concat_axis=0, tiled=True)  19.6 us
    all_to_all x1, blocking collectives, on_device(): tiles = lax.all_to_all(parts.reshape(n_fs, own, cols), FS, 0, 0, tiled=True)  17.6 us
    all_to_all x1, starting transfers between devices, on_device(): basis_mine = lax.all_to_all(copies, FS, 0, 0, tiled=True).reshape(d, half)  15.3 us
    all_to_all x1, waiting for transfers between devices, on_device(): basis_mine = lax.all_to_all(copies, FS, 0, 0, tiled=True).reshape(d, half)  11.9 us
    all_to_all x1, blocking collectives, on_device(): lax.all_to_all(packs, NEAR, 0, 0, tiled=True).reshape(near * per, cols)  8.93 us
    ppermute x1, starting transfers between devices, on_device(): basis_other = lax.ppermute(basis_mine, 'tp_1', pair)  8.46 us
    all_to_all x1, starting transfers between devices, on_device(): squares = lax.all_to_all(local, TP, 0, 0, tiled=True)  7.08 us
    pallas_call x1, Pallas kernels, on_device(): pl.pallas_call(final_kernel, out_shape=outs[:4] + (shape((d, kc), bf16),...  5.17 us
  transfers between devices with their start and end apart: 4, of which 2 were waited for; matrix products, arithmetic and copies ran while one was open for 4% of the time, Pallas kernels for 4%

profile of v2, /device:TPU:1, one launch (start us, length us, event | category | flops | bytes accessed | tf_op | source)
XLA Modules:
  0.0 123.2 jit_solution(12413626260406782902)
XLA Ops:
  7.2 0.0 all-gather.2.cloned.1.call-start
  7.2 1.7 %pack.1 = (bf16[4,40,384]{2,1,0:T(8,128)(2,1)S(1)}, bf16[64,32,128]{2,1,0:T(8,128)(2,1)}) custom-call(s32[1]{0:T(128)} %bitcast.core, f32[32,128]{1,0:T(8,128)} %mk_h.1, f32[32,256]{1,0:T(8,128)} %mv_h.1, f32[4,128]{1,0:T(4,128)} %fk_h.1, f32[4,256]{1,0:T(4,128)} %fv_h.1, f32[4,128]{1,0:T(4,128)} %sk_h.1, f32[4,256]{1,0:T(4,128)} %sv_h.1, ...), custom_call_target="tpu_custom_call" | custom-call | tf_op jit(solution)/shard_map/pack/pallas_call | solution.py:214
  8.9 8.9 %all_to_all.25 = bf16[4,40,384]{2,1,0:T(8,128)(2,1)} all-to-all(bf16[4,40,384]{2,1,0:T(8,128)(2,1)S(1)} %get-tuple-element.24), channel_id=1, replica_groups=mesh['fs_0'=4,'fs_1'=2,'fs_2'=4,'fs_3'=2,'tp_0'=4,'tp_1'=2] {'fs_1','fs_3'}, dimensions={0} | all-to-all | bytes 245760 | tf_op jit(solution)/shard_map/all_to_all | solution.py:222
  17.8 0.0 all-gather.2.cloned.1.call-update
  17.8 15.3 %all-to-all-start = ((bf16[64,32,128]{2,1,0:T(8,128)(2,1)}), bf16[64,32,128]{2,1,0:T(8,128)(2,1)}, u32[]{:S(2)}, u32[]{:S(2)}) async-start(bf16[64,32,128]{2,1,0:T(8,128)(2,1)} %get-tuple-element.19), calls=%async_computation | async-start | bytes 1048576 | tf_op jit(solution)/shard_map/all_to_all | solution.py:228
  33.2 4.3 %subtract_convert_fusion = (bf16[384,2048]{1,0:T(8,128)(2,1)S(1)}, bf16[384,2048]{1,0:T(8,128)(2,1)S(1)}) fusion(bf16[1024,2048]{1,0:T(8,128)(2,1)} %param.10, bf16[1024,256]{1,0:T(8,128)(2,1)} %param.12, bf16[1024,128]{1,0:T(8,128)(2,1)} %param.11), kind=kOutput, calls=%fused_computation | convolution fusion | flops 1615331328 | bytes 8126464 | tf_op jit(solution)/shard_map/dot_general | solution.py:231
  37.5 11.9 %all-to-all-done = bf16[64,32,128]{2,1,0:T(8,128)(2,1)} async-done(((bf16[64,32,128]{2,1,0:T(8,128)(2,1)}), bf16[64,32,128]{2,1,0:T(8,128)(2,1)}, u32[]{:S(2)}, u32[]{:S(2)}) %all-to-all-start) | async-done | bytes 524320 | tf_op jit(solution)/shard_map/all_to_all | solution.py:228
  49.4 8.5 %collective-permute-start = (bf16[2048,128]{1,0:T(8,128)(2,1)}, bf16[2048,128]{1,0:T(8,128)(2,1)S(1)}, u32[]{:S(2)}, u32[]{:S(2)}) collective-permute-start(bf16[2048,128]{1,0:T(8,128)(2,1)} %bitcast.1.basis.b_mine_h), channel_id=1, source_target_pairs={{0,1},{1,0},{2,3},{3,2},{4,5},{5,4},{6,7},{7,6},{8,9},{9,8},{10,11... | collective-permute-start | bytes 1572872 | tf_op jit(solution)/shard_map/ppermute | solution.py:235
  57.9 2.1 %project_mine.1.mine = f32[128,384]{1,0:T(8,128)S(1)} custom-call(bf16[384,2048]{1,0:T(8,128)(2,1)S(1)} %get-tuple-element.20.hi, bf16[384,2048]{1,0:T(8,128)(2,1)S(1)} %get-tuple-element.21.lo, bf16[2048,128]{1,0:T(8,128)(2,1)} %bitcast.1.basis.b_mine_h), custom_call_target="tpu_custom_call" | custom-call | flops 402653184 | bytes 3670016 | tf_op jit(solution)/shard_map/project_mine/pallas_call | solution.py:237
  60.0 0.0 collective-permute-done.basis
  60.0 1.1 project_other.1
  61.0 0.1 reshape.40
  61.1 17.6 %all_to_all.26 = bf16[64,4,384]{2,1,0:T(4,128)(2,1)S(1)} all-to-all(bf16[64,4,384]{2,1,0:T(4,128)(2,1)S(1)} %reshape.40), channel_id=1, replica_groups=mesh['fs_0'=4,'fs_1'=2,'fs_2'=4,'fs_3'=2,'tp_0'=4,'tp_1'=2] {'fs_0','fs_..., dimensions={0} | all-to-all | bytes 393216 | tf_op jit(solution)/shard_map/all_to_all | solution.py:256
  78.7 0.1 convert_reduce_fusion.own_low_h
  78.8 0.1 broadcast_in_dim.3
  78.9 19.6 %all_to_all.27 = bf16[64,4,384]{2,1,0:T(4,128)(2,1)S(1)} all-to-all(bf16[64,4,384]{2,1,0:T(4,128)(2,1)S(1)} %broadcast_in_dim.3), channel_id=1, replica_groups=mesh['fs_0'=4,'fs_1'=2,'fs_2'=4,'fs_3'=2,'tp_0'=4,'tp_1'=2] {'fs_0','fs_..., dimensions={0} | all-to-all | bytes 393216 | tf_op jit(solution)/shard_map/all_to_all | solution.py:197
  98.5 0.1 reshape.41.low.low_h
  98.5 0.8 squares.1
  99.4 7.1 %all-to-all-start.3 = ((f32[8,8,128]{2,1,0:T(8,128)}), f32[8,8,128]{2,1,0:T(8,128)S(1)}, u32[]{:S(2)}, u32[]{:S(2)}) async-start(f32[8,8,128]{2,1,0:T(8,128)} %squares.1), calls=%async_computation.3 | async-start | bytes 65536 | tf_op jit(solution)/shard_map/all_to_all | solution.py:268
  106.5 0.0 all-gather.2.cloned.1.call-done
  106.5 1.5 %prep.1 = (bf16[256,384]{1,0:T(8,128)(2,1)S(1)}, bf16[256,384]{1,0:T(8,128)(2,1)S(1)}) custom-call(bf16[4,4,2,2,40,384]{5,4,3,2,1,0:T(8,128)(2,1)} %bitcast.5), custom_call_target="tpu_custom_call" | custom-call | flops 201326592 | bytes 1966080 | tf_op jit(solution)/shard_map/prep/pallas_call | solution.py:269
  107.9 3.2 %all-to-all-done.3.squares = f32[8,8,128]{2,1,0:T(8,128)S(1)} async-done(((f32[8,8,128]{2,1,0:T(8,128)}), f32[8,8,128]{2,1,0:T(8,128)S(1)}, u32[]{:S(2)}, u32[]{:S(2)}) %all-to-all-start.3) | async-done | bytes 32800 | tf_op jit(solution)/shard_map/all_to_all | solution.py:268
  111.2 5.2 %update.1 = (f32[32,128]{1,0:T(8,128)}, f32[32,256]{1,0:T(8,128)}, f32[32,128]{1,0:T(8,128)}, f32[32,256]{1,0:T(8,128)}, bf16[2048,128]{1,0:T(8,128)(2,1)}, /*in...) custom-call(s32[1]{0:T(128)} %bitcast.core, ...), custom_call_target="tpu_custom_call" | custom-call | tf_op jit(solution)/shard_map/update/pallas_call | solution.py:286
  (1 shorter events, 0.0 us)
Async XLA Ops:
  7.2 99.3 %all-gather.2.cloned.1.call-start = ((), (), s32[]{:S(2)}) async-start(), calls=%async_computation.5 | async-start | bytes 2088960 | tf_op jit(solution)/shard_map/all_gather | solution.py:223
  17.8 31.6 %all-to-all-start = ((bf16[64,32,128]{2,1,0:T(8,128)(2,1)}), bf16[64,32,128]{2,1,0:T(8,128)(2,1)}, u32[]{:S(2)}, u32[]{:S(2)}) async-start(bf16[64,32,128]{2,1,0:T(8,128)(2,1)} %get-tuple-element.19), calls=%async_computation | async-start | bytes 1048576 | tf_op jit(solution)/shard_map/all_to_all | solution.py:228
  49.4 10.6 %collective-permute-start = (bf16[2048,128]{1,0:T(8,128)(2,1)}, bf16[2048,128]{1,0:T(8,128)(2,1)S(1)}, u32[]{:S(2)}, u32[]{:S(2)}) collective-permute-start(bf16[2048,128]{1,0:T(8,128)(2,1)} %bitcast.1.basis.b_mine_h), channel_id=1, source_target_pairs={{0,1},{1,0},{2,3},{3,2},{4,5},{5,4},{6,7},{7,6},{8,9},{9,8},{10,11... | collective-permute-start | bytes 1572872 | tf_op jit(solution)/shard_map/ppermute | solution.py:235
  99.4 11.8 %all-to-all-start.3 = ((f32[8,8,128]{2,1,0:T(8,128)}), f32[8,8,128]{2,1,0:T(8,128)S(1)}, u32[]{:S(2)}, u32[]{:S(2)}) async-start(f32[8,8,128]{2,1,0:T(8,128)} %squares.1), calls=%async_computation.3 | async-start | bytes 65536 | tf_op jit(solution)/shard_map/all_to_all | solution.py:268
Sparse Core Ops, SparseCore 0:
  18.0 74.4 all-gather.1

commit v3 on v0

v3 whole, which is shorter than its diff:
```python
import jax
import jax.numpy as jnp
from jax import lax
from jax.experimental import pallas as pl
from jax.experimental.pallas import tpu as pltpu
from jax.sharding import Mesh
from jax.sharding import PartitionSpec as P

DK = 1024
DV = 2048
R = 256
FS = ("fs_0", "fs_1")
TP = ("tp_0", "tp_1")

learn_rate = 0.05
beta_first = 0.9
beta_second = 0.9
epsilon = 1e-08
norm_eps = 1e-06


f32 = jnp.float32
bf16 = jnp.bfloat16
VMEM = pl.BlockSpec(memory_space=pltpu.VMEM)
SMEM = pl.BlockSpec(memory_space=pltpu.SMEM)
ANY = pl.BlockSpec(memory_space=pl.ANY)
HBM = pl.BlockSpec(memory_space=pltpu.HBM)


def shape(dims, dtype):
    return jax.ShapeDtypeStruct(dims, dtype)


def cost(flops, moved):
    return pl.CostEstimate(flops=flops, bytes_accessed=moved, transcendentals=0)


def in_hbm(array):
    return pltpu.with_memory_space_constraint(array, pltpu.HBM)


def limit(mib):
    return pltpu.CompilerParams(vmem_limit_bytes=mib * 1024 * 1024)


def dot(a, b):
    return jnp.dot(a, b, preferred_element_type=f32)


def pack_kernel(mk, mv, fk, fv, sk, sv, pack):
    rows, kc = mk.shape
    pack[:rows, :kc] = mk[...].astype(bf16)
    pack[:rows, kc:] = mv[...].astype(bf16)
    pack[rows:, :kc] = jnp.concatenate([fk[...], sk[...]], axis=0).astype(bf16)
    pack[rows:, kc:] = jnp.concatenate([fv[...], sv[...]], axis=0).astype(bf16)


def copies_kernel(core, basis, copies):
    half = copies.shape[2]
    mine = jnp.where(core[0] == 0, basis[:, :half].astype(f32), basis[:, half:].astype(f32))
    copies[...] = jnp.broadcast_to(mine.astype(bf16)[None], copies.shape)


def project_kernel(hi, lo, basis, out):
    b = basis[...]
    out[...] = (dot(hi[...], b) + dot(lo[...], b)).T


def project_both_kernel(core, hi, lo, basis, mine, out, kept, sem):
    half = mine.shape[0]
    keep = pltpu.make_async_copy(basis, kept, sem)
    keep.start()
    b = basis[...]
    at = pl.multiple_of(core[0] * half, half)
    other = pl.multiple_of((1 - core[0]) * half, half)
    out[pl.ds(at, half), :] = mine[...]
    out[pl.ds(other, half), :] = (dot(hi[...], b) + dot(lo[...], b)).T
    keep.wait()


def squares_kernel(low, out):
    x = low[...].astype(f32)
    out[...] = jnp.broadcast_to(jnp.sum(x * x, keepdims=True)[None], out.shape)


def moments(low, scale, first, second):
    scaled = low * scale
    new_first = beta_first * first + (1.0 - beta_first) * scaled
    new_second = beta_second * second + (1.0 - beta_second) * scaled * scaled
    return new_first, new_second


def prep_kernel(
    core, mine, other, basis, mk, mv, fk, fv, sk, sv,
    full_basis, own_basis, master, first, second,
    mk_v, mv_v, fk_v, fv_v, sk_v, sv_v, sems,
):
    kc = mk.shape[1]
    half = mine.shape[1]
    at = pl.multiple_of(core[0] * half, half)
    at_other = pl.multiple_of((1 - core[0]) * half, half)
    loads = [
        pltpu.make_async_copy(mine, full_basis.at[:, pl.ds(at, half)], sems.at[0]),
        pltpu.make_async_copy(other, full_basis.at[:, pl.ds(at_other, half)], sems.at[1]),
        pltpu.make_async_copy(basis, own_basis, sems.at[2]),
        pltpu.make_async_copy(mk, mk_v, sems.at[3]),
        pltpu.make_async_copy(mv, mv_v, sems.at[4]),
        pltpu.make_async_copy(fk, fk_v, sems.at[5]),
        pltpu.make_async_copy(fv, fv_v, sems.at[6]),
        pltpu.make_async_copy(sk, sk_v, sems.at[7]),
        pltpu.make_async_copy(sv, sv_v, sems.at[8]),
    ]
    for load in loads:
        load.start()
    for load in loads:
        load.wait()
    master[:, :kc] = mk_v[...]
    master[:, kc:] = mv_v[...]
    first[:, :kc] = fk_v[...]
    first[:, kc:] = fv_v[...]
    second[:, :kc] = sk_v[...]
    second[:, kc:] = sv_v[...]


def final_kernel(
    squares, low, own_low, full_basis, basis, master, first, second, gathered,
    step_k, step_v, new_k, new_v, copy_k, copy_v, nf_k, ns_k, nf_v, ns_v,
    mom, masters, out_k, out_v,
    step_ks, step_vs, new_ks, new_vs, nf_ks, ns_ks, nf_vs, ns_vs, mom_sem, master_sem, out_sem, own_sem,
):
    n_fs, per, cols = mom.shape
    rows = master.shape[0]
    kc = step_k.shape[1]
    chunks = master_sem.shape[0]
    group = n_fs // chunks
    size = group * rows
    load = pltpu.make_async_copy(gathered.at[:, pl.ds(rows, per), :], mom, mom_sem)
    load.start()
    loads = []
    for k in range(chunks):
        at = pl.ds(k * group, group)
        source = gathered.at[at, pl.ds(0, rows), :]
        loads.append(pltpu.make_async_copy(source, masters.at[at], master_sem.at[k]))
        loads[k].start()

    stores = []

    def store(source, target, sem):
        stores.append(pltpu.make_async_copy(source, target, sem))
        stores[-1].start()

    total = jnp.sum(squares[...], axis=0)[:1, :1]
    scale = 1.0 / jnp.sqrt(total / (R * (DK + DV)) + norm_eps)
    nf, ns = moments(own_low[...], scale, first[...], second[...])
    nf_ks[...] = nf[:, :kc]
    nf_vs[...] = nf[:, kc:]
    ns_ks[...] = ns[:, :kc]
    ns_vs[...] = ns[:, kc:]

    own = per // 2
    i = lax.broadcasted_iota(jnp.int32, (n_fs * own, n_fs * per), 0)
    j = lax.broadcasted_iota(jnp.int32, (n_fs * own, n_fs * per), 1)
    at_first = (i // own) * per + i % own
    pick_first = jnp.where(j == at_first, 1.0, 0.0).astype(bf16)
    pick_second = jnp.where(j == at_first + own, 1.0, 0.0).astype(bf16)
    load.wait()
    both = mom[...].reshape(n_fs * per, cols)
    nf, ns = moments(low[...].astype(f32), scale, dot(pick_first, both), dot(pick_second, both))
    direction = (nf / (jnp.sqrt(ns) + epsilon)).astype(bf16)

    for k in range(chunks):
        at = pl.ds(k * size, size)
        step = dot(full_basis[at, :], direction)
        loads[k].wait()
        old = masters[pl.ds(k * group, group)].astype(f32).reshape(size, cols)
        copy = (old - learn_rate * step).astype(bf16)
        out_k[at, :] = copy[:, :kc]
        out_v[at, :] = copy[:, kc:]
        store(out_k.at[at], copy_k.at[at], out_sem.at[0, k])
        store(out_v.at[at], copy_v.at[at], out_sem.at[1, k])
        if k == 0:
            step = dot(basis[...], direction)
            step_ks[...] = step[:, :kc]
            step_vs[...] = step[:, kc:]
            new = master[...] - learn_rate * step
            new_ks[...] = new[:, :kc]
            new_vs[...] = new[:, kc:]
            sources = (step_ks, step_vs, new_ks, new_vs, nf_ks, ns_ks, nf_vs, ns_vs)
            targets = (step_k, step_v, new_k, new_v, nf_k, ns_k, nf_v, ns_v)
            for n in range(len(sources)):
                store(sources[n], targets[n], own_sem.at[n])
    for item in stores:
        item.wait()


def to_everyone(array, axis):
    copies = jnp.broadcast_to(array, (lax.axis_size(axis), *array.shape))
    return lax.all_to_all(copies, axis, split_axis=0, concat_axis=0, tiled=True)


def on_device(normed, key_cot, value_cot, basis, mk, mv, fk, sk, fv, sv):
    kc = key_cot.shape[1]
    cols = kc + value_cot.shape[1]
    rows = basis.shape[0]
    d = normed.shape[1]
    own = fk.shape[0]
    n_fs = lax.axis_size(FS)
    n_tp = lax.axis_size(TP)
    half = R // 2
    core = lax.axis_index("tp_1").astype(jnp.int32).reshape(1)
    per = rows + 2 * own
    pair = [(0, 1), (1, 0)]

    pack = pl.pallas_call(
        pack_kernel,
        out_shape=shape((per, cols), bf16),
        in_specs=[VMEM] * 6,
        out_specs=VMEM,
        compiler_params=limit(24),
        name="pack",
    )(*(in_hbm(x) for x in (mk, mv, fk, fv, sk, sv)))
    gathered = lax.all_gather(pack, FS, axis=0, tiled=True).reshape(n_fs, per, cols)
    copies = pl.pallas_call(
        copies_kernel,
        out_shape=shape((n_fs, rows, half), bf16),
        in_specs=[SMEM, VMEM],
        out_specs=VMEM,
        compiler_params=limit(24),
        name="copies",
    )(core, in_hbm(basis))
    basis_mine = lax.all_to_all(copies, FS, 0, 0, tiled=True).reshape(d, half)

    cot = jnp.concatenate([key_cot, value_cot], axis=1)
    grad = lax.dot_general(cot, normed, (((0,), (0,)), ((), ())), preferred_element_type=f32)
    hi = grad.astype(bf16)
    lo = (grad - hi.astype(f32)).astype(bf16)
    basis_mine, hi, lo = lax.optimization_barrier((basis_mine, hi, lo))
    basis_other = lax.ppermute(basis_mine, "tp_1", pair)
    project_cost = cost(4 * d * half * cols, 4 * d * cols + 2 * d * half)
    low_mine = pl.pallas_call(
        project_kernel,
        out_shape=shape((half, cols), f32),
        in_specs=[VMEM] * 3,
        out_specs=VMEM,
        cost_estimate=project_cost,
        compiler_params=limit(12),
        name="project_mine",
    )(hi, lo, basis_mine)
    parts, basis_other = pl.pallas_call(
        project_both_kernel,
        out_shape=(shape((R, cols), f32), pltpu.HBM((d, half), bf16)),
        in_specs=[SMEM] + [VMEM] * 4,
        out_specs=(VMEM, HBM),
        scratch_shapes=[pltpu.SemaphoreType.DMA],
        cost_estimate=project_cost,
        compiler_params=limit(12),
        name="project_other",
    )(core, hi, lo, basis_other, low_mine)
    tiles = lax.all_to_all(parts.reshape(n_fs, own, cols), FS, 0, 0, tiled=True)
    own_low = jnp.sum(tiles.astype(f32), axis=0)

    all_low = to_everyone(own_low.astype(bf16), FS).reshape(R, cols)
    local = pl.pallas_call(
        squares_kernel,
        out_shape=shape((n_tp, 8, 128), f32),
        in_specs=[VMEM],
        out_specs=VMEM,
        compiler_params=limit(4),
        name="squares",
    )(all_low)
    squares = lax.all_to_all(local, TP, 0, 0, tiled=True)
    vc = cols - kc
    small = ((rows, kc), (rows, vc)) * 2 + ((own, kc), (own, kc), (own, vc), (own, vc))
    held = pl.pallas_call(
        prep_kernel,
        out_shape=(
            shape((d, R), bf16),
            shape((rows, R), bf16),
            shape((rows, cols), f32),
            shape((own, cols), f32),
            shape((own, cols), f32),
        ),
        in_specs=[SMEM] + [ANY] * 9,
        out_specs=(VMEM,) * 5,
        scratch_shapes=[
            pltpu.VMEM((rows, kc), f32),
            pltpu.VMEM((rows, vc), f32),
            pltpu.VMEM((own, kc), f32),
            pltpu.VMEM((own, vc), f32),
            pltpu.VMEM((own, kc), f32),
            pltpu.VMEM((own, vc), f32),
            pltpu.SemaphoreType.DMA((9,)),
        ],
        cost_estimate=cost(4 * R * 2 * R * cols, 4 * d * R),
        compiler_params=limit(24),
        name="prep",
    )(core, *(in_hbm(x) for x in (basis_mine, basis_other, basis, mk, mv, fk, fv, sk, sv)))

    chunks = 8
    outs = tuple(shape(dims, f32) for dims in small)
    return pl.pallas_call(
        final_kernel,
        out_shape=outs[:4] + (shape((d, kc), bf16), shape((d, vc), bf16)) + outs[4:],
        in_specs=[VMEM] * 8 + [ANY],
        out_specs=(HBM,) * 10,
        scratch_shapes=[
            pltpu.VMEM((n_fs, 2 * own, cols), bf16),
            pltpu.VMEM((n_fs, rows, cols), bf16),
            pltpu.VMEM((d, kc), bf16),
            pltpu.VMEM((d, vc), bf16),
        ]
        + [pltpu.VMEM(dims, f32) for dims in small]
        + [
            pltpu.SemaphoreType.DMA,
            pltpu.SemaphoreType.DMA((chunks,)),
            pltpu.SemaphoreType.DMA((2, chunks)),
            pltpu.SemaphoreType.DMA((8,)),
        ],
        compiler_params=limit(32),
        name="update",
    )(squares, all_low, own_low, *held, in_hbm(gathered))


def solution(mesh):
    names = (*FS, *TP)
    torus = Mesh(mesh.devices.reshape(8, 8, 4, 2), names)
    split = P(FS, TP)
    in_specs = (P(FS, None), split, split, P(FS, None)) + (split,) * 6
    out_specs = (split,) * 4 + (P(None, TP),) * 2 + (split,) * 4
    return jax.shard_map(
        on_device, mesh=torus, in_specs=in_specs, out_specs=out_specs, check_vma=False
    )
```

time: 126 us -> 118 us (0.937)
  starting transfers between devices: 36.4 us -> 30.3 us
  blocking collectives: 41.1 us -> 39 us
    ppermute x1 -> x0, starting transfers between devices: 4.01 us -> none  [on_device(): other_pack = lax.ppermute(pack, 'fs_2', pair)]
    ppermute x1, starting transfers between devices: 7.8 us -> 5.49 us  [on_device(): basis_other = lax.ppermute(basis_mine, 'tp_1', pair)]
    all_to_all x1, blocking collectives: 20.9 us -> 18.8 us  [to_everyone(): return lax.all_to_all(copies, axis, split_axis=0, concat_axis=0, tiled=True)]
    all_to_all x1, waiting for transfers between devices: 11.5 us -> 12.8 us  [on_device(): basis_mine = lax.all_to_all(copies, FS, 0, 0, tiled=True).reshape(d, half)]
    ppermute x1 -> x0, waiting for transfers between devices: 1.26 us -> none  [on_device(): other_pack = lax.ppermute(pack, 'fs_2', pair)]
  transfers between devices with their start and end apart: 5 -> 4, of which waited for: 3 -> 2; matrix products, arithmetic and copies ran while one was open for 4% -> 4% of each run, Pallas kernels for 4% -> 6%
where the time goes in v3:
time: 118 us; the launch traced here: 117 us
  blocking collectives  39 us (33%)
  starting transfers between devices  30.3 us (26%)
  waiting for transfers between devices  16.2 us (14%)
  between operations  14.1 us (12%)
  Pallas kernels  13.2 us (11%)
  matrix products  4.28 us (4%)
    all_to_all x1, blocking collectives, on_device(): tiles = lax.all_to_all(parts.reshape(n_fs, own, cols), FS, 0, 0, tiled=True)  20.3 us
    all_to_all x1, blocking collectives, to_everyone(): return lax.all_to_all(copies, axis, split_axis=0, concat_axis=0, tiled=True)  18.8 us
    all_to_all x1, starting transfers between devices, on_device(): basis_mine = lax.all_to_all(copies, FS, 0, 0, tiled=True).reshape(d, half)  17.4 us
    all_to_all x1, waiting for transfers between devices, on_device(): basis_mine = lax.all_to_all(copies, FS, 0, 0, tiled=True).reshape(d, half)  12.8 us
    all_to_all x1, starting transfers between devices, on_device(): squares = lax.all_to_all(local, TP, 0, 0, tiled=True)  7.43 us
    ppermute x1, starting transfers between devices, on_device(): basis_other = lax.ppermute(basis_mine, 'tp_1', pair)  5.49 us
    pallas_call x1, Pallas kernels, on_device(): pl.pallas_call(final_kernel, out_shape=outs[:4] + (shape((d, kc), bf16),...  4.94 us
    dot_general x1, matrix products, on_device(): lax.dot_general(cot, normed, (((0,), (0,)), ((), ())), preferred_element_...  4.28 us
  transfers between devices with their start and end apart: 4, of which 2 were waited for; matrix products, arithmetic and copies ran while one was open for 4% of the time, Pallas kernels for 6%

profile of v3, /device:TPU:1, one launch (start us, length us, event | category | flops | bytes accessed | tf_op | source)
XLA Modules:
  0.0 117.5 jit_solution(12092272532240351891)
XLA Ops:
  7.2 0.0 all-gather.2.cloned.1.call-start
  7.2 1.4 %pack.1 = bf16[40,384]{1,0:T(8,128)(2,1)} custom-call(f32[32,128]{1,0:T(8,128)} %mk.3, f32[32,256]{1,0:T(8,128)} %mv.3, f32[4,128]{1,0:T(4,128)} %fk.3, f32[4,256]{1,0:T(4,128)} %fv.3, f32[4,128]{1,0:T(4,128)} %sk.3, f32[4,256]{1,0:T(4,128)} %sv.3), custom_call_target="tpu_custom_call" | custom-call | tf_op jit(solution)/shard_map/pack/pallas_call | solution.py:214
  8.6 0.0 all-gather.2.cloned.1.call-update
  8.6 1.6 %copies.1 = bf16[64,32,128]{2,1,0:T(8,128)(2,1)} custom-call(s32[1]{0:T(128)} %bitcast.core, bf16[32,256]{1,0:T(8,128)(2,1)} %basis.3), custom_call_target="tpu_custom_call" | custom-call | tf_op jit(solution)/shard_map/copies/pallas_call | solution.py:223
  10.2 17.4 %all-to-all-start = ((bf16[64,32,128]{2,1,0:T(8,128)(2,1)}), bf16[64,32,128]{2,1,0:T(8,128)(2,1)}, u32[]{:S(2)}, u32[]{:S(2)}) async-start(bf16[64,32,128]{2,1,0:T(8,128)(2,1)} %copies.1), calls=%async_computation | async-start | bytes 1048576 | tf_op jit(solution)/shard_map/all_to_all | solution.py:231
  27.6 4.3 %subtract_convert_fusion = (bf16[384,2048]{1,0:T(8,128)(2,1)S(1)}, bf16[384,2048]{1,0:T(8,128)(2,1)S(1)}) fusion(bf16[1024,2048]{1,0:T(8,128)(2,1)} %param.10, bf16[1024,256]{1,0:T(8,128)(2,1)} %param.12, bf16[1024,128]{1,0:T(8,128)(2,1)} %param.11), kind=kOutput, calls=%fused_computation | convolution fusion | flops 1615331328 | bytes 8126464 | tf_op jit(solution)/shard_map/dot_general | solution.py:234
  31.9 12.8 %all-to-all-done = bf16[64,32,128]{2,1,0:T(8,128)(2,1)} async-done(((bf16[64,32,128]{2,1,0:T(8,128)(2,1)}), bf16[64,32,128]{2,1,0:T(8,128)(2,1)}, u32[]{:S(2)}, u32[]{:S(2)}) %all-to-all-start) | async-done | bytes 524320 | tf_op jit(solution)/shard_map/all_to_all | solution.py:231
  44.7 5.5 %collective-permute-start = (bf16[2048,128]{1,0:T(8,128)(2,1)}, bf16[2048,128]{1,0:T(8,128)(2,1)S(1)}, u32[]{:S(2)}, u32[]{:S(2)}) collective-permute-start(bf16[2048,128]{1,0:T(8,128)(2,1)} %bitcast.1.basis.mine), channel_id=1, source_target_pairs={{0,1},{1,0},{2,3},{3,2},{4,5},{5,4},{6,7},{7,6},{8,9},{9,8},{10,11... | collective-permute-start | bytes 1572872 | tf_op jit(solution)/shard_map/ppermute | solution.py:238
  50.2 2.1 %project_mine.1.mine = f32[128,384]{1,0:T(8,128)S(1)} custom-call(bf16[384,2048]{1,0:T(8,128)(2,1)S(1)} %get-tuple-element.20.hi, bf16[384,2048]{1,0:T(8,128)(2,1)S(1)} %get-tuple-element.21.lo, bf16[2048,128]{1,0:T(8,128)(2,1)} %bitcast.1.basis.mine), custom_call_target="tpu_custom_call" | custom-call | flops 402653184 | bytes 3670016 | tf_op jit(solution)/shard_map/project_mine/pallas_call | solution.py:240
  52.3 0.0 collective-permute-done.basis
  52.3 1.1 project_other.1
  53.3 0.1 reshape.37
  53.5 20.3 %all_to_all.20 = f32[64,4,384]{2,1,0:T(4,128)S(1)} all-to-all(f32[64,4,384]{2,1,0:T(4,128)S(1)} %reshape.37), channel_id=1, replica_groups=mesh['fs_0'=8,'fs_1'=8,'tp_0'=4,'tp_1'=2] {'fs_0','fs_1'}, dimensions={0} | all-to-all | bytes 786432 | tf_op jit(solution)/shard_map/all_to_all | solution.py:259
  73.7 0.1 reduce_sum.9.own_low
  73.8 0.1 broadcast_in_dim.3
  73.9 18.8 %all_to_all.21 = bf16[64,4,384]{2,1,0:T(4,128)(2,1)S(1)} all-to-all(bf16[64,4,384]{2,1,0:T(4,128)(2,1)S(1)} %broadcast_in_dim.3), channel_id=1, replica_groups=mesh['fs_0'=8,'fs_1'=8,'tp_0'=4,'tp_1'=2] {'fs_0','fs_1'}, dimensions={0} | all-to-all | bytes 393216 | tf_op jit(solution)/shard_map/all_to_all | solution.py:198
  92.6 0.1 reshape.38.low
  92.7 0.8 squares.1
  93.5 7.4 %all-to-all-start.3 = ((f32[8,8,128]{2,1,0:T(8,128)}), f32[8,8,128]{2,1,0:T(8,128)S(1)}, u32[]{:S(2)}, u32[]{:S(2)}) async-start(f32[8,8,128]{2,1,0:T(8,128)} %squares.1), calls=%async_computation.3 | async-start | bytes 65536 | tf_op jit(solution)/shard_map/all_to_all | solution.py:271
  101.0 1.3 %prep.1 = (bf16[2048,256]{1,0:T(8,128)(2,1)S(1)}, bf16[32,256]{1,0:T(8,128)(2,1)S(1)}, f32[32,384]{1,0:T(8,128)S(1)}, f32[4,384]{1,0:T(4,128)S(1)}, f32[4,384]{1,0:T(4,128)S(1)}) custom-call(s32[1]{0:T(128)} %bitcast.core, bf16[2048,128]{1,0:T(8,128)(2,1)} %bitcast.1.basis.mine, bf16[2048,128]{1,0:T(8,128)(2,1)} %get-tuple-element.24.other, ...), custom_call_target="tpu_custom_call" | custom-call | flops 201326592 | bytes 2097152 | tf_op jit(solution)/shard_map/prep/pallas_call | solution.py:274
  102.3 3.4 %all-to-all-done.3.squares = f32[8,8,128]{2,1,0:T(8,128)S(1)} async-done(((f32[8,8,128]{2,1,0:T(8,128)}), f32[8,8,128]{2,1,0:T(8,128)S(1)}, u32[]{:S(2)}, u32[]{:S(2)}) %all-to-all-start.3) | async-done | bytes 32800 | tf_op jit(solution)/shard_map/all_to_all | solution.py:271
  105.7 0.0 all-gather.2.cloned.1.call-done
  105.7 4.9 %update.1 = (f32[32,128]{1,0:T(8,128)}, f32[32,256]{1,0:T(8,128)}, f32[32,128]{1,0:T(8,128)}, f32[32,256]{1,0:T(8,128)}, bf16[2048,128]{1,0:T(8,128)(2,1)}, /*in...) custom-call(f32[8,8,128]{2,1,0:T(8,128)S(1)} %all-to-all-done.3.squares, ...), custom_call_target="tpu_custom_call" | custom-call | tf_op jit(solution)/shard_map/update/pallas_call | solution.py:301
  (1 shorter events, 0.0 us)
Async XLA Ops:
  7.2 98.5 %all-gather.2.cloned.1.call-start = ((), (), s32[]{:S(2)}) async-start(), calls=%async_computation.4 | async-start | bytes 1996800 | tf_op jit(solution)/shard_map/all_gather | solution.py:222
  10.2 34.5 %all-to-all-start = ((bf16[64,32,128]{2,1,0:T(8,128)(2,1)}), bf16[64,32,128]{2,1,0:T(8,128)(2,1)}, u32[]{:S(2)}, u32[]{:S(2)}) async-start(bf16[64,32,128]{2,1,0:T(8,128)(2,1)} %copies.1), calls=%async_computation | async-start | bytes 1048576 | tf_op jit(solution)/shard_map/all_to_all | solution.py:231
  44.7 7.6 %collective-permute-start = (bf16[2048,128]{1,0:T(8,128)(2,1)}, bf16[2048,128]{1,0:T(8,128)(2,1)S(1)}, u32[]{:S(2)}, u32[]{:S(2)}) collective-permute-start(bf16[2048,128]{1,0:T(8,128)(2,1)} %bitcast.1.basis.mine), channel_id=1, source_target_pairs={{0,1},{1,0},{2,3},{3,2},{4,5},{5,4},{6,7},{7,6},{8,9},{9,8},{10,11... | collective-permute-start | bytes 1572872 | tf_op jit(solution)/shard_map/ppermute | solution.py:238
  93.5 12.1 %all-to-all-start.3 = ((f32[8,8,128]{2,1,0:T(8,128)}), f32[8,8,128]{2,1,0:T(8,128)S(1)}, u32[]{:S(2)}, u32[]{:S(2)}) async-start(f32[8,8,128]{2,1,0:T(8,128)} %squares.1), calls=%async_computation.3 | async-start | bytes 65536 | tf_op jit(solution)/shard_map/all_to_all | solution.py:271
Sparse Core Ops, SparseCore 0:
  11.6 87.9 all-gather.1

commit v4 on v3

--- a/solution.py
+++ b/solution.py
@@ -47,23 +47,29 @@
     return jnp.dot(a, b, preferred_element_type=f32)
 
 
-def pack_kernel(mk, mv, fk, fv, sk, sv, pack):
+def pack_kernel(core, mk, mv, fk, fv, sk, sv, basis, pack, copies):
     rows, kc = mk.shape
+    half = copies.shape[2]
+    mine = jnp.where(core[0] == 0, basis[:, :half].astype(f32), basis[:, half:].astype(f32))
+    copies[...] = jnp.broadcast_to(mine.astype(bf16)[None], copies.shape)
     pack[:rows, :kc] = mk[...].astype(bf16)
     pack[:rows, kc:] = mv[...].astype(bf16)
     pack[rows:, :kc] = jnp.concatenate([fk[...], sk[...]], axis=0).astype(bf16)
     pack[rows:, kc:] = jnp.concatenate([fv[...], sv[...]], axis=0).astype(bf16)
 
 
-def copies_kernel(core, basis, copies):
-    half = copies.shape[2]
-    mine = jnp.where(core[0] == 0, basis[:, :half].astype(f32), basis[:, half:].astype(f32))
-    copies[...] = jnp.broadcast_to(mine.astype(bf16)[None], copies.shape)
-
-
-def project_kernel(hi, lo, basis, out):
-    b = basis[...]
-    out[...] = (dot(hi[...], b) + dot(lo[...], b)).T
+def project_kernel(hi, lo, basis, out, held, sems):
+    chunks = sems.shape[0]
+    depth = held.shape[0] // chunks
+    spans = [pl.ds(k * depth, depth) for k in range(chunks)]
+    loads = [pltpu.make_async_copy(basis.at[at], held.at[at], sems.at[k]) for k, at in enumerate(spans)]
+    for load in loads:
+        load.start()
+    total = jnp.zeros((hi.shape[0], held.shape[1]), f32)
+    for load, at in zip(loads, spans):
+        load.wait()
+        total += dot(hi[:, at], held[at, :]) + dot(lo[:, at], held[at, :])
+    out[...] = total.T
 
 
 def project_both_kernel(core, hi, lo, basis, mine, out, kept, sem):
@@ -211,23 +217,15 @@
     per = rows + 2 * own
     pair = [(0, 1), (1, 0)]
 
-    pack = pl.pallas_call(
+    pack, copies = pl.pallas_call(
         pack_kernel,
-        out_shape=shape((per, cols), bf16),
-        in_specs=[VMEM] * 6,
-        out_specs=VMEM,
+        out_shape=(shape((per, cols), bf16), shape((n_fs, rows, half), bf16)),
+        in_specs=[SMEM] + [VMEM] * 7,
+        out_specs=(VMEM, VMEM),
         compiler_params=limit(24),
         name="pack",
-    )(*(in_hbm(x) for x in (mk, mv, fk, fv, sk, sv)))
+    )(core, *(in_hbm(x) for x in (mk, mv, fk, fv, sk, sv, basis)))
     gathered = lax.all_gather(pack, FS, axis=0, tiled=True).reshape(n_fs, per, cols)
-    copies = pl.pallas_call(
-        copies_kernel,
-        out_shape=shape((n_fs, rows, half), bf16),
-        in_specs=[SMEM, VMEM],
-        out_specs=VMEM,
-        compiler_params=limit(24),
-        name="copies",
-    )(core, in_hbm(basis))
     basis_mine = lax.all_to_all(copies, FS, 0, 0, tiled=True).reshape(d, half)
 
     cot = jnp.concatenate([key_cot, value_cot], axis=1)
@@ -240,12 +238,13 @@
     low_mine = pl.pallas_call(
         project_kernel,
         out_shape=shape((half, cols), f32),
-        in_specs=[VMEM] * 3,
+        in_specs=[VMEM] * 2 + [ANY],
         out_specs=VMEM,
+        scratch_shapes=[pltpu.VMEM((d, half), bf16), pltpu.SemaphoreType.DMA((4,))],
         cost_estimate=project_cost,
         compiler_params=limit(12),
         name="project_mine",
-    )(hi, lo, basis_mine)
+    )(hi, lo, in_hbm(basis_mine))
     parts, basis_other = pl.pallas_call(
         project_both_kernel,
         out_shape=(shape((R, cols), f32), pltpu.HBM((d, half), bf16)),

time: 118 us -> 118 us (level)
  the two profiles are of different devices: /device:TPU:1 before, /device:TPU:10 now
where the time goes in v4:
time: 118 us; the launch traced here: 117 us
  blocking collectives  42 us (36%)
  starting transfers between devices  23.5 us (20%)
  waiting for transfers between devices  20.2 us (17%)
  between operations  14.1 us (12%)
  Pallas kernels  12.8 us (11%)
  matrix products  4.28 us (4%)
    all_to_all x1, blocking collectives, on_device(): tiles = lax.all_to_all(parts.reshape(n_fs, own, cols), FS, 0, 0, tiled=True)  22.2 us
    all_to_all x1, blocking collectives, to_everyone(): return lax.all_to_all(copies, axis, split_axis=0, concat_axis=0, tiled=True)  19.8 us
    all_to_all x1, starting transfers between devices, on_device(): basis_mine = lax.all_to_all(copies, FS, 0, 0, tiled=True).reshape(d, half)  16.8 us
    all_to_all x1, waiting for transfers between devices, on_device(): basis_mine = lax.all_to_all(copies, FS, 0, 0, tiled=True).reshape(d, half)  15.4 us
    pallas_call x1, Pallas kernels, on_device(): pl.pallas_call(final_kernel, out_shape=outs[:4] + (shape((d, kc), bf16),...  4.94 us
    all_to_all x1, starting transfers between devices, on_device(): squares = lax.all_to_all(local, TP, 0, 0, tiled=True)  4.8 us
    dot_general x1, matrix products, on_device(): lax.dot_general(cot, normed, (((0,), (0,)), ((), ())), preferred_element_...  4.28 us
    pallas_call x1, Pallas kernels, on_device(): pl.pallas_call(project_kernel, out_shape=shape((half, cols), f32), in_spe...  2.99 us
  transfers between devices with their start and end apart: 4, of which 3 were waited for; matrix products, arithmetic and copies ran while one was open for 4% of the time, Pallas kernels for 5%

profile of v4, /device:TPU:10, one launch (start us, length us, event | category | flops | bytes accessed | tf_op | source)
XLA Modules:
  0.0 117.2 jit_solution(15849285197936838874)
XLA Ops:
  7.2 0.0 all-gather.2.cloned.1.call-start
  7.2 1.7 %pack.1 = (bf16[40,384]{1,0:T(8,128)(2,1)}, bf16[64,32,128]{2,1,0:T(8,128)(2,1)}) custom-call(s32[1]{0:T(128)} %bitcast.core, f32[32,128]{1,0:T(8,128)} %mk.3, f32[32,256]{1,0:T(8,128)} %mv.3, f32[4,128]{1,0:T(4,128)} %fk.3, f32[4,256]{1,0:T(4,128)} %fv.3, f32[4,128]{1,0:T(4,128)} %sk.3, f32[4,256]{1,0:T(4,128)} %sv.3, bf16[32,256]{1,0:T(8,128)(2,1)} %basis.3), custom_call_target="tpu_custom_call" | custom-call | tf_op jit(solution)/shard_map/pack/pallas_call | solution.py:220
  8.9 0.0 all-gather.2.cloned.1.call-update
  8.9 16.8 %all-to-all-start = ((bf16[64,32,128]{2,1,0:T(8,128)(2,1)}), bf16[64,32,128]{2,1,0:T(8,128)(2,1)}, u32[]{:S(2)}, u32[]{:S(2)}) async-start(bf16[64,32,128]{2,1,0:T(8,128)(2,1)} %get-tuple-element.22), calls=%async_computation | async-start | bytes 1048576 | tf_op jit(solution)/shard_map/all_to_all | solution.py:229
  25.7 4.3 %subtract_convert_fusion = (bf16[384,2048]{1,0:T(8,128)(2,1)S(1)}, bf16[384,2048]{1,0:T(8,128)(2,1)S(1)}) fusion(bf16[1024,2048]{1,0:T(8,128)(2,1)} %param.10, bf16[1024,256]{1,0:T(8,128)(2,1)} %param.12, bf16[1024,128]{1,0:T(8,128)(2,1)} %param.11), kind=kOutput, calls=%fused_computation | convolution fusion | flops 1615331328 | bytes 8126464 | tf_op jit(solution)/shard_map/dot_general | solution.py:232
  30.0 15.4 %all-to-all-done = bf16[64,32,128]{2,1,0:T(8,128)(2,1)} async-done(((bf16[64,32,128]{2,1,0:T(8,128)(2,1)}), bf16[64,32,128]{2,1,0:T(8,128)(2,1)}, u32[]{:S(2)}, u32[]{:S(2)}) %all-to-all-start) | async-done | bytes 524320 | tf_op jit(solution)/shard_map/all_to_all | solution.py:229
  45.4 1.9 %collective-permute-start = (bf16[2048,128]{1,0:T(8,128)(2,1)}, bf16[2048,128]{1,0:T(8,128)(2,1)S(1)}, u32[]{:S(2)}, u32[]{:S(2)}) collective-permute-start(bf16[2048,128]{1,0:T(8,128)(2,1)} %bitcast.1.basis.mine), channel_id=1, source_target_pairs={{0,1},{1,0},{2,3},{3,2},{4,5},{5,4},{6,7},{7,6},{8,9},{9,8},{10,11... | collective-permute-start | bytes 1572872 | tf_op jit(solution)/shard_map/ppermute | solution.py:236
  47.3 3.0 %project_mine.1.mine = f32[128,384]{1,0:T(8,128)S(1)} custom-call(bf16[384,2048]{1,0:T(8,128)(2,1)S(1)} %get-tuple-element.23.hi, bf16[384,2048]{1,0:T(8,128)(2,1)S(1)} %get-tuple-element.24.lo, bf16[2048,128]{1,0:T(8,128)(2,1)} %bitcast.1.basis.mine), custom_call_target="tpu_custom_call" | custom-call | flops 402653184 | bytes 3670016 | tf_op jit(solution)/shard_map/project_mine/pallas_call | solution.py:238
  50.3 0.0 collective-permute-done.basis
  50.3 1.1 project_other.1
  51.4 0.1 reshape.37
  51.5 22.2 %all_to_all.20 = f32[64,4,384]{2,1,0:T(4,128)S(1)} all-to-all(f32[64,4,384]{2,1,0:T(4,128)S(1)} %reshape.37), channel_id=1, replica_groups=mesh['fs_0'=8,'fs_1'=8,'tp_0'=4,'tp_1'=2] {'fs_0','fs_1'}, dimensions={0} | all-to-all | bytes 786432 | tf_op jit(solution)/shard_map/all_to_all | solution.py:258
  73.7 0.1 reduce_sum.9.own_low
  73.8 0.1 broadcast_in_dim.3
  73.9 19.8 %all_to_all.21 = bf16[64,4,384]{2,1,0:T(4,128)(2,1)S(1)} all-to-all(bf16[64,4,384]{2,1,0:T(4,128)(2,1)S(1)} %broadcast_in_dim.3), channel_id=1, replica_groups=mesh['fs_0'=8,'fs_1'=8,'tp_0'=4,'tp_1'=2] {'fs_0','fs_1'}, dimensions={0} | all-to-all | bytes 393216 | tf_op jit(solution)/shard_map/all_to_all | solution.py:204
  93.7 0.1 reshape.38.low
  93.7 0.8 squares.1
  94.5 4.8 %all-to-all-start.3 = ((f32[8,8,128]{2,1,0:T(8,128)}), f32[8,8,128]{2,1,0:T(8,128)S(1)}, u32[]{:S(2)}, u32[]{:S(2)}) async-start(f32[8,8,128]{2,1,0:T(8,128)} %squares.1), calls=%async_computation.3 | async-start | bytes 65536 | tf_op jit(solution)/shard_map/all_to_all | solution.py:270
  99.3 1.3 %prep.1 = (bf16[2048,256]{1,0:T(8,128)(2,1)S(1)}, bf16[32,256]{1,0:T(8,128)(2,1)S(1)}, f32[32,384]{1,0:T(8,128)S(1)}, f32[4,384]{1,0:T(4,128)S(1)}, f32[4,384]{1,0:T(4,128)S(1)}) custom-call(s32[1]{0:T(128)} %bitcast.core, bf16[2048,128]{1,0:T(8,128)(2,1)} %bitcast.1.basis.mine, bf16[2048,128]{1,0:T(8,128)(2,1)} %get-tuple-element.27.other, ...), custom_call_target="tpu_custom_call" | custom-call | flops 201326592 | bytes 2097152 | tf_op jit(solution)/shard_map/prep/pallas_call | solution.py:273
  100.7 2.7 %all-to-all-done.3.squares = f32[8,8,128]{2,1,0:T(8,128)S(1)} async-done(((f32[8,8,128]{2,1,0:T(8,128)}), f32[8,8,128]{2,1,0:T(8,128)S(1)}, u32[]{:S(2)}, u32[]{:S(2)}) %all-to-all-start.3) | async-done | bytes 32800 | tf_op jit(solution)/shard_map/all_to_all | solution.py:270
  103.3 2.0 %all-gather.2.cloned.1.call-done = bf16[2560,384]{1,0:T(8,128)(2,1)} async-done(((bf16[40,384]{1,0:T(8,128)(2,1)}), bf16[2560,384]{1,0:T(8,128)(2,1)}) %all-gather.2.cloned.1.call-update) | async-done | bytes 1966096 | tf_op jit(solution)/shard_map/all_gather | solution.py:228
  105.4 4.9 %update.1 = (f32[32,128]{1,0:T(8,128)}, f32[32,256]{1,0:T(8,128)}, f32[32,128]{1,0:T(8,128)}, f32[32,256]{1,0:T(8,128)}, bf16[2048,128]{1,0:T(8,128)(2,1)}, /*in...) custom-call(f32[8,8,128]{2,1,0:T(8,128)S(1)} %all-to-all-done.3.squares, ...), custom_call_target="tpu_custom_call" | custom-call | tf_op jit(solution)/shard_map/update/pallas_call | solution.py:300
  (1 shorter events, 0.0 us)
Async XLA Ops:
  7.2 98.2 %all-gather.2.cloned.1.call-start = ((), (), s32[]{:S(2)}) async-start(), calls=%async_computation.4 | async-start | bytes 1996800 | tf_op jit(solution)/shard_map/all_gather | solution.py:228
  8.9 36.5 %all-to-all-start = ((bf16[64,32,128]{2,1,0:T(8,128)(2,1)}), bf16[64,32,128]{2,1,0:T(8,128)(2,1)}, u32[]{:S(2)}, u32[]{:S(2)}) async-start(bf16[64,32,128]{2,1,0:T(8,128)(2,1)} %get-tuple-element.22), calls=%async_computation | async-start | bytes 1048576 | tf_op jit(solution)/shard_map/all_to_all | solution.py:229
  45.4 4.9 %collective-permute-start = (bf16[2048,128]{1,0:T(8,128)(2,1)}, bf16[2048,128]{1,0:T(8,128)(2,1)S(1)}, u32[]{:S(2)}, u32[]{:S(2)}) collective-permute-start(bf16[2048,128]{1,0:T(8,128)(2,1)} %bitcast.1.basis.mine), channel_id=1, source_target_pairs={{0,1},{1,0},{2,3},{3,2},{4,5},{5,4},{6,7},{7,6},{8,9},{9,8},{10,11... | collective-permute-start | bytes 1572872 | tf_op jit(solution)/shard_map/ppermute | solution.py:236
  94.5 8.8 %all-to-all-start.3 = ((f32[8,8,128]{2,1,0:T(8,128)}), f32[8,8,128]{2,1,0:T(8,128)S(1)}, u32[]{:S(2)}, u32[]{:S(2)}) async-start(f32[8,8,128]{2,1,0:T(8,128)} %squares.1), calls=%async_computation.3 | async-start | bytes 65536 | tf_op jit(solution)/shard_map/all_to_all | solution.py:270
Sparse Core Ops, SparseCore 0:
  11.6 93.7 all-gather.1

commit v5 on v4

--- a/solution.py
+++ b/solution.py
@@ -58,18 +58,9 @@
     pack[rows:, kc:] = jnp.concatenate([fv[...], sv[...]], axis=0).astype(bf16)
 
 
-def project_kernel(hi, lo, basis, out, held, sems):
-    chunks = sems.shape[0]
-    depth = held.shape[0] // chunks
-    spans = [pl.ds(k * depth, depth) for k in range(chunks)]
-    loads = [pltpu.make_async_copy(basis.at[at], held.at[at], sems.at[k]) for k, at in enumerate(spans)]
-    for load in loads:
-        load.start()
-    total = jnp.zeros((hi.shape[0], held.shape[1]), f32)
-    for load, at in zip(loads, spans):
-        load.wait()
-        total += dot(hi[:, at], held[at, :]) + dot(lo[:, at], held[at, :])
-    out[...] = total.T
+def project_kernel(hi, lo, basis, out):
+    b = basis[...]
+    out[...] = (dot(hi[...], b) + dot(lo[...], b)).T
 
 
 def project_both_kernel(core, hi, lo, basis, mine, out, kept, sem):
@@ -79,8 +70,8 @@
     b = basis[...]
     at = pl.multiple_of(core[0] * half, half)
     other = pl.multiple_of((1 - core[0]) * half, half)
-    out[pl.ds(at, half), :] = mine[...]
-    out[pl.ds(other, half), :] = (dot(hi[...], b) + dot(lo[...], b)).T
+    out[pl.ds(at, half), :] = mine[...].astype(bf16)
+    out[pl.ds(other, half), :] = (dot(hi[...], b) + dot(lo[...], b)).T.astype(bf16)
     keep.wait()
 
 
@@ -238,16 +229,15 @@
     low_mine = pl.pallas_call(
         project_kernel,
         out_shape=shape((half, cols), f32),
-        in_specs=[VMEM] * 2 + [ANY],
+        in_specs=[VMEM] * 3,
         out_specs=VMEM,
-        scratch_shapes=[pltpu.VMEM((d, half), bf16), pltpu.SemaphoreType.DMA((4,))],
         cost_estimate=project_cost,
         compiler_params=limit(12),
         name="project_mine",
-    )(hi, lo, in_hbm(basis_mine))
+    )(hi, lo, basis_mine)
     parts, basis_other = pl.pallas_call(
         project_both_kernel,
-        out_shape=(shape((R, cols), f32), pltpu.HBM((d, half), bf16)),
+        out_shape=(shape((R, cols), bf16), pltpu.HBM((d, half), bf16)),
         in_specs=[SMEM] + [VMEM] * 4,
         out_specs=(VMEM, HBM),
         scratch_shapes=[pltpu.SemaphoreType.DMA],

time: 118 us -> 118 us (level)
  the two profiles are of different devices: /device:TPU:10 before, /device:TPU:2 now
where the time goes in v5:
time: 118 us; the launch traced here: 117 us
  blocking collectives  38 us (32%)
  waiting for transfers between devices  25.1 us (21%)
  starting transfers between devices  23.5 us (20%)
  between operations  14.1 us (12%)
  Pallas kernels  11.9 us (10%)
  matrix products  4.28 us (4%)
    all_to_all x1, blocking collectives, on_device(): tiles = lax.all_to_all(parts.reshape(n_fs, own, cols), FS, 0, 0, tiled=True)  19.3 us
    all_to_all x1, blocking collectives, to_everyone(): return lax.all_to_all(copies, axis, split_axis=0, concat_axis=0, tiled=True)  18.7 us
    all_to_all x1, starting transfers between devices, on_device(): basis_mine = lax.all_to_all(copies, FS, 0, 0, tiled=True).reshape(d, half)  16.9 us
    all_to_all x1, waiting for transfers between devices, on_device(): basis_mine = lax.all_to_all(copies, FS, 0, 0, tiled=True).reshape(d, half)  15.5 us
    all_gather x1, waiting for transfers between devices, on_device(): lax.all_gather(pack, FS, axis=0, tiled=True).reshape(n_fs, per, cols)  6.9 us
    pallas_call x1, Pallas kernels, on_device(): pl.pallas_call(final_kernel, out_shape=outs[:4] + (shape((d, kc), bf16),...  4.94 us
    all_to_all x1, starting transfers between devices, on_device(): squares = lax.all_to_all(local, TP, 0, 0, tiled=True)  4.7 us
    dot_general x1, matrix products, on_device(): lax.dot_general(cot, normed, (((0,), (0,)), ((), ())), preferred_element_...  4.28 us
  transfers between devices with their start and end apart: 4, of which 3 were waited for; matrix products, arithmetic and copies ran while one was open for 4% of the time, Pallas kernels for 5%

profile of v5, /device:TPU:2, one launch (start us, length us, event | category | flops | bytes accessed | tf_op | source)
XLA Modules:
  0.0 117.1 jit_solution(17614400666028652066)
XLA Ops:
  7.2 0.0 all-gather.2.cloned.1.call-start
  7.2 1.7 %pack.1 = (bf16[40,384]{1,0:T(8,128)(2,1)}, bf16[64,32,128]{2,1,0:T(8,128)(2,1)}) custom-call(s32[1]{0:T(128)} %bitcast.core, f32[32,128]{1,0:T(8,128)} %mk.3, f32[32,256]{1,0:T(8,128)} %mv.3, f32[4,128]{1,0:T(4,128)} %fk.3, f32[4,256]{1,0:T(4,128)} %fv.3, f32[4,128]{1,0:T(4,128)} %sk.3, f32[4,256]{1,0:T(4,128)} %sv.3, bf16[32,256]{1,0:T(8,128)(2,1)} %basis.3), custom_call_target="tpu_custom_call" | custom-call | tf_op jit(solution)/shard_map/pack/pallas_call | solution.py:211
  8.9 0.0 all-gather.2.cloned.1.call-update
  8.9 16.9 %all-to-all-start = ((bf16[64,32,128]{2,1,0:T(8,128)(2,1)}), bf16[64,32,128]{2,1,0:T(8,128)(2,1)}, u32[]{:S(2)}, u32[]{:S(2)}) async-start(bf16[64,32,128]{2,1,0:T(8,128)(2,1)} %get-tuple-element.22), calls=%async_computation | async-start | bytes 1048576 | tf_op jit(solution)/shard_map/all_to_all | solution.py:220
  25.8 4.3 %subtract_convert_fusion = (bf16[384,2048]{1,0:T(8,128)(2,1)S(1)}, bf16[384,2048]{1,0:T(8,128)(2,1)S(1)}) fusion(bf16[1024,2048]{1,0:T(8,128)(2,1)} %param.10, bf16[1024,256]{1,0:T(8,128)(2,1)} %param.12, bf16[1024,128]{1,0:T(8,128)(2,1)} %param.11), kind=kOutput, calls=%fused_computation | convolution fusion | flops 1615331328 | bytes 8126464 | tf_op jit(solution)/shard_map/dot_general | solution.py:223
  30.1 15.5 %all-to-all-done = bf16[64,32,128]{2,1,0:T(8,128)(2,1)} async-done(((bf16[64,32,128]{2,1,0:T(8,128)(2,1)}), bf16[64,32,128]{2,1,0:T(8,128)(2,1)}, u32[]{:S(2)}, u32[]{:S(2)}) %all-to-all-start) | async-done | bytes 524320 | tf_op jit(solution)/shard_map/all_to_all | solution.py:220
  45.5 1.9 %collective-permute-start = (bf16[2048,128]{1,0:T(8,128)(2,1)}, bf16[2048,128]{1,0:T(8,128)(2,1)S(1)}, u32[]{:S(2)}, u32[]{:S(2)}) collective-permute-start(bf16[2048,128]{1,0:T(8,128)(2,1)} %bitcast.1.basis.mine), channel_id=1, source_target_pairs={{0,1},{1,0},{2,3},{3,2},{4,5},{5,4},{6,7},{7,6},{8,9},{9,8},{10,11... | collective-permute-start | bytes 1572872 | tf_op jit(solution)/shard_map/ppermute | solution.py:227
  47.4 2.1 %project_mine.1.mine = f32[128,384]{1,0:T(8,128)S(1)} custom-call(bf16[384,2048]{1,0:T(8,128)(2,1)S(1)} %get-tuple-element.23.hi, bf16[384,2048]{1,0:T(8,128)(2,1)S(1)} %get-tuple-element.24.lo, bf16[2048,128]{1,0:T(8,128)(2,1)} %bitcast.1.basis.mine), custom_call_target="tpu_custom_call" | custom-call | flops 402653184 | bytes 3670016 | tf_op jit(solution)/shard_map/project_mine/pallas_call | solution.py:229
  49.5 0.0 collective-permute-done.basis
  49.5 1.1 project_other.1
  50.6 0.1 reshape.37
  50.7 19.3 %all_to_all.20 = bf16[64,4,384]{2,1,0:T(4,128)(2,1)S(1)} all-to-all(bf16[64,4,384]{2,1,0:T(4,128)(2,1)S(1)} %reshape.37), channel_id=1, replica_groups=mesh['fs_0'=8,'fs_1'=8,'tp_0'=4,'tp_1'=2] {'fs_0','fs_1'}, dimensions={0} | all-to-all | bytes 393216 | tf_op jit(solution)/shard_map/all_to_all | solution.py:248
  69.9 0.1 convert_reduce_fusion.own_low
  70.1 0.1 broadcast_in_dim.3
  70.1 18.7 %all_to_all.21 = bf16[64,4,384]{2,1,0:T(4,128)(2,1)S(1)} all-to-all(bf16[64,4,384]{2,1,0:T(4,128)(2,1)S(1)} %broadcast_in_dim.3), channel_id=1, replica_groups=mesh['fs_0'=8,'fs_1'=8,'tp_0'=4,'tp_1'=2] {'fs_0','fs_1'}, dimensions={0} | all-to-all | bytes 393216 | tf_op jit(solution)/shard_map/all_to_all | solution.py:195
  88.8 0.1 reshape.38.low
  88.9 0.8 squares.1
  89.7 4.7 %all-to-all-start.3 = ((f32[8,8,128]{2,1,0:T(8,128)}), f32[8,8,128]{2,1,0:T(8,128)S(1)}, u32[]{:S(2)}, u32[]{:S(2)}) async-start(f32[8,8,128]{2,1,0:T(8,128)} %squares.1), calls=%async_computation.3 | async-start | bytes 65536 | tf_op jit(solution)/shard_map/all_to_all | solution.py:260
  94.4 1.3 %prep.1 = (bf16[2048,256]{1,0:T(8,128)(2,1)S(1)}, bf16[32,256]{1,0:T(8,128)(2,1)S(1)}, f32[32,384]{1,0:T(8,128)S(1)}, f32[4,384]{1,0:T(4,128)S(1)}, f32[4,384]{1,0:T(4,128)S(1)}) custom-call(s32[1]{0:T(128)} %bitcast.core, bf16[2048,128]{1,0:T(8,128)(2,1)} %bitcast.1.basis.mine, bf16[2048,128]{1,0:T(8,128)(2,1)} %get-tuple-element.27.other, ...), custom_call_target="tpu_custom_call" | custom-call | flops 201326592 | bytes 2097152 | tf_op jit(solution)/shard_map/prep/pallas_call | solution.py:263
  95.7 2.7 %all-to-all-done.3.squares = f32[8,8,128]{2,1,0:T(8,128)S(1)} async-done(((f32[8,8,128]{2,1,0:T(8,128)}), f32[8,8,128]{2,1,0:T(8,128)S(1)}, u32[]{:S(2)}, u32[]{:S(2)}) %all-to-all-start.3) | async-done | bytes 32800 | tf_op jit(solution)/shard_map/all_to_all | solution.py:260
  98.4 6.9 %all-gather.2.cloned.1.call-done = bf16[2560,384]{1,0:T(8,128)(2,1)} async-done(((bf16[40,384]{1,0:T(8,128)(2,1)}), bf16[2560,384]{1,0:T(8,128)(2,1)}) %all-gather.2.cloned.1.call-update) | async-done | bytes 1966096 | tf_op jit(solution)/shard_map/all_gather | solution.py:219
  105.3 4.9 %update.1 = (f32[32,128]{1,0:T(8,128)}, f32[32,256]{1,0:T(8,128)}, f32[32,128]{1,0:T(8,128)}, f32[32,256]{1,0:T(8,128)}, bf16[2048,128]{1,0:T(8,128)(2,1)}, /*in...) custom-call(f32[8,8,128]{2,1,0:T(8,128)S(1)} %all-to-all-done.3.squares, ...), custom_call_target="tpu_custom_call" | custom-call | tf_op jit(solution)/shard_map/update/pallas_call | solution.py:290
  (1 shorter events, 0.0 us)
Async XLA Ops:
  7.2 98.1 %all-gather.2.cloned.1.call-start = ((), (), s32[]{:S(2)}) async-start(), calls=%async_computation.4 | async-start | bytes 1996800 | tf_op jit(solution)/shard_map/all_gather | solution.py:219
  8.9 36.6 %all-to-all-start = ((bf16[64,32,128]{2,1,0:T(8,128)(2,1)}), bf16[64,32,128]{2,1,0:T(8,128)(2,1)}, u32[]{:S(2)}, u32[]{:S(2)}) async-start(bf16[64,32,128]{2,1,0:T(8,128)(2,1)} %get-tuple-element.22), calls=%async_computation | async-start | bytes 1048576 | tf_op jit(solution)/shard_map/all_to_all | solution.py:220
  45.5 4.0 %collective-permute-start = (bf16[2048,128]{1,0:T(8,128)(2,1)}, bf16[2048,128]{1,0:T(8,128)(2,1)S(1)}, u32[]{:S(2)}, u32[]{:S(2)}) collective-permute-start(bf16[2048,128]{1,0:T(8,128)(2,1)} %bitcast.1.basis.mine), channel_id=1, source_target_pairs={{0,1},{1,0},{2,3},{3,2},{4,5},{5,4},{6,7},{7,6},{8,9},{9,8},{10,11... | collective-permute-start | bytes 1572872 | tf_op jit(solution)/shard_map/ppermute | solution.py:227
  89.7 8.7 %all-to-all-start.3 = ((f32[8,8,128]{2,1,0:T(8,128)}), f32[8,8,128]{2,1,0:T(8,128)S(1)}, u32[]{:S(2)}, u32[]{:S(2)}) async-start(f32[8,8,128]{2,1,0:T(8,128)} %squares.1), calls=%async_computation.3 | async-start | bytes 65536 | tf_op jit(solution)/shard_map/all_to_all | solution.py:260
Sparse Core Ops, SparseCore 0:
  11.6 93.6 all-gather.1

commit v6 on v5

--- a/solution.py
+++ b/solution.py
@@ -70,8 +70,8 @@
     b = basis[...]
     at = pl.multiple_of(core[0] * half, half)
     other = pl.multiple_of((1 - core[0]) * half, half)
-    out[pl.ds(at, half), :] = mine[...].astype(bf16)
-    out[pl.ds(other, half), :] = (dot(hi[...], b) + dot(lo[...], b)).T.astype(bf16)
+    out[pl.ds(at, half), :] = mine[...]
+    out[pl.ds(other, half), :] = (dot(hi[...], b) + dot(lo[...], b)).T
     keep.wait()
 
 
@@ -122,22 +122,20 @@
 def final_kernel(
     squares, low, own_low, full_basis, basis, master, first, second, gathered,
     step_k, step_v, new_k, new_v, copy_k, copy_v, nf_k, ns_k, nf_v, ns_v,
-    mom, masters, out_k, out_v,
-    step_ks, step_vs, new_ks, new_vs, nf_ks, ns_ks, nf_vs, ns_vs, mom_sem, master_sem, out_sem, own_sem,
+    held, out_k, out_v,
+    step_ks, step_vs, new_ks, new_vs, nf_ks, ns_ks, nf_vs, ns_vs, in_sem, out_sem, own_sem,
 ):
-    n_fs, per, cols = mom.shape
+    n_fs, block, cols = held.shape
     rows = master.shape[0]
+    per = block - rows
     kc = step_k.shape[1]
-    chunks = master_sem.shape[0]
+    chunks = in_sem.shape[0]
     group = n_fs // chunks
     size = group * rows
-    load = pltpu.make_async_copy(gathered.at[:, pl.ds(rows, per), :], mom, mom_sem)
-    load.start()
     loads = []
     for k in range(chunks):
         at = pl.ds(k * group, group)
-        source = gathered.at[at, pl.ds(0, rows), :]
-        loads.append(pltpu.make_async_copy(source, masters.at[at], master_sem.at[k]))
+        loads.append(pltpu.make_async_copy(gathered.at[at], held.at[at], in_sem.at[k]))
         loads[k].start()
 
     stores = []
@@ -160,16 +158,16 @@
     at_first = (i // own) * per + i % own
     pick_first = jnp.where(j == at_first, 1.0, 0.0).astype(bf16)
     pick_second = jnp.where(j == at_first + own, 1.0, 0.0).astype(bf16)
-    load.wait()
-    both = mom[...].reshape(n_fs * per, cols)
+    for load in loads:
+        load.wait()
+    both = held[:, rows:].reshape(n_fs * per, cols)
     nf, ns = moments(low[...].astype(f32), scale, dot(pick_first, both), dot(pick_second, both))
     direction = (nf / (jnp.sqrt(ns) + epsilon)).astype(bf16)
 
     for k in range(chunks):
         at = pl.ds(k * size, size)
         step = dot(full_basis[at, :], direction)
-        loads[k].wait()
-        old = masters[pl.ds(k * group, group)].astype(f32).reshape(size, cols)
+        old = held[pl.ds(k * group, group), :rows].astype(f32).reshape(size, cols)
         copy = (old - learn_rate * step).astype(bf16)
         out_k[at, :] = copy[:, :kc]
         out_v[at, :] = copy[:, kc:]
@@ -237,7 +235,7 @@
     )(hi, lo, basis_mine)
     parts, basis_other = pl.pallas_call(
         project_both_kernel,
-        out_shape=(shape((R, cols), bf16), pltpu.HBM((d, half), bf16)),
+        out_shape=(shape((R, cols), f32), pltpu.HBM((d, half), bf16)),
         in_specs=[SMEM] + [VMEM] * 4,
         out_specs=(VMEM, HBM),
         scratch_shapes=[pltpu.SemaphoreType.DMA],
@@ -246,7 +244,7 @@
         name="project_other",
     )(core, hi, lo, basis_other, low_mine)
     tiles = lax.all_to_all(parts.reshape(n_fs, own, cols), FS, 0, 0, tiled=True)
-    own_low = jnp.sum(tiles.astype(f32), axis=0)
+    own_low = jnp.sum(tiles, axis=0)
 
     all_low = to_everyone(own_low.astype(bf16), FS).reshape(R, cols)
     local = pl.pallas_call(
@@ -285,7 +283,7 @@
         name="prep",
     )(core, *(in_hbm(x) for x in (basis_mine, basis_other, basis, mk, mv, fk, fv, sk, sv)))
 
-    chunks = 8
+    chunks = 2
     outs = tuple(shape(dims, f32) for dims in small)
     return pl.pallas_call(
         final_kernel,
@@ -293,14 +291,12 @@
         in_specs=[VMEM] * 8 + [ANY],
         out_specs=(HBM,) * 10,
         scratch_shapes=[
-            pltpu.VMEM((n_fs, 2 * own, cols), bf16),
-            pltpu.VMEM((n_fs, rows, cols), bf16),
+            pltpu.VMEM((n_fs, per, cols), bf16),
             pltpu.VMEM((d, kc), bf16),
             pltpu.VMEM((d, vc), bf16),
         ]
         + [pltpu.VMEM(dims, f32) for dims in small]
         + [
-            pltpu.SemaphoreType.DMA,
             pltpu.SemaphoreType.DMA((chunks,)),
             pltpu.SemaphoreType.DMA((2, chunks)),
             pltpu.SemaphoreType.DMA((8,)),

time: 118 us -> 118 us (level)
  the two profiles are of different devices: /device:TPU:2 before, /device:TPU:8 now
where the time goes in v6:
time: 118 us
  blocking collectives  41.4 us (35%)
  waiting for transfers between devices  24.1 us (20%)
  starting transfers between devices  23 us (19%)
  between operations  14.1 us (12%)
  Pallas kernels  10.7 us (9%)
  matrix products  4.28 us (4%)
    all_to_all x1, blocking collectives, on_device(): tiles = lax.all_to_all(parts.reshape(n_fs, own, cols), FS, 0, 0, tiled=True)  22.2 us
    all_to_all x1, blocking collectives, to_everyone(): return lax.all_to_all(copies, axis, split_axis=0, concat_axis=0, tiled=True)  19.1 us
    all_to_all x1, starting transfers between devices, on_device(): basis_mine = lax.all_to_all(copies, FS, 0, 0, tiled=True).reshape(d, half)  16.8 us
    all_to_all x1, waiting for transfers between devices, on_device(): basis_mine = lax.all_to_all(copies, FS, 0, 0, tiled=True).reshape(d, half)  15.4 us
    all_gather x1, waiting for transfers between devices, on_device(): lax.all_gather(pack, FS, axis=0, tiled=True).reshape(n_fs, per, cols)  4.51 us
    dot_general x1, matrix products, on_device(): lax.dot_general(cot, normed, (((0,), (0,)), ((), ())), preferred_element_...  4.28 us
    all_to_all x1, starting transfers between devices, on_device(): squares = lax.all_to_all(local, TP, 0, 0, tiled=True)  4.28 us
    all_to_all x1, waiting for transfers between devices, on_device(): squares = lax.all_to_all(local, TP, 0, 0, tiled=True)  4.14 us
  transfers between devices with their start and end apart: 4, of which 3 were waited for; matrix products, arithmetic and copies ran while one was open for 4% of the time, Pallas kernels for 4%

profile of v6, /device:TPU:8, one launch (start us, length us, event | category | flops | bytes accessed | tf_op | source)
XLA Modules:
  0.0 117.9 jit_solution(4836269800381802328)
XLA Ops:
  7.2 0.0 all-gather.2.cloned.1.call-start
  7.2 1.7 %pack.1 = (bf16[40,384]{1,0:T(8,128)(2,1)}, bf16[64,32,128]{2,1,0:T(8,128)(2,1)}) custom-call(s32[1]{0:T(128)} %bitcast.core, f32[32,128]{1,0:T(8,128)} %mk.3, f32[32,256]{1,0:T(8,128)} %mv.3, f32[4,128]{1,0:T(4,128)} %fk.3, f32[4,256]{1,0:T(4,128)} %fv.3, f32[4,128]{1,0:T(4,128)} %sk.3, f32[4,256]{1,0:T(4,128)} %sv.3, bf16[32,256]{1,0:T(8,128)(2,1)} %basis.3), custom_call_target="tpu_custom_call" | custom-call | tf_op jit(solution)/shard_map/pack/pallas_call | solution.py:209
  8.9 0.0 all-gather.2.cloned.1.call-update
  8.9 16.8 %all-to-all-start = ((bf16[64,32,128]{2,1,0:T(8,128)(2,1)}), bf16[64,32,128]{2,1,0:T(8,128)(2,1)}, u32[]{:S(2)}, u32[]{:S(2)}) async-start(bf16[64,32,128]{2,1,0:T(8,128)(2,1)} %get-tuple-element.22), calls=%async_computation | async-start | bytes 1048576 | tf_op jit(solution)/shard_map/all_to_all | solution.py:218
  25.7 4.3 %subtract_convert_fusion = (bf16[384,2048]{1,0:T(8,128)(2,1)S(1)}, bf16[384,2048]{1,0:T(8,128)(2,1)S(1)}) fusion(bf16[1024,2048]{1,0:T(8,128)(2,1)} %param.10, bf16[1024,256]{1,0:T(8,128)(2,1)} %param.12, bf16[1024,128]{1,0:T(8,128)(2,1)} %param.11), kind=kOutput, calls=%fused_computation | convolution fusion | flops 1615331328 | bytes 8126464 | tf_op jit(solution)/shard_map/dot_general | solution.py:221
  30.0 15.4 %all-to-all-done = bf16[64,32,128]{2,1,0:T(8,128)(2,1)} async-done(((bf16[64,32,128]{2,1,0:T(8,128)(2,1)}), bf16[64,32,128]{2,1,0:T(8,128)(2,1)}, u32[]{:S(2)}, u32[]{:S(2)}) %all-to-all-start) | async-done | bytes 524320 | tf_op jit(solution)/shard_map/all_to_all | solution.py:218
  45.4 1.9 %collective-permute-start = (bf16[2048,128]{1,0:T(8,128)(2,1)}, bf16[2048,128]{1,0:T(8,128)(2,1)S(1)}, u32[]{:S(2)}, u32[]{:S(2)}) collective-permute-start(bf16[2048,128]{1,0:T(8,128)(2,1)} %bitcast.1.basis.mine), channel_id=1, source_target_pairs={{0,1},{1,0},{2,3},{3,2},{4,5},{5,4},{6,7},{7,6},{8,9},{9,8},{10,11... | collective-permute-start | bytes 1572872 | tf_op jit(solution)/shard_map/ppermute | solution.py:225
  47.3 2.1 %project_mine.1.mine = f32[128,384]{1,0:T(8,128)S(1)} custom-call(bf16[384,2048]{1,0:T(8,128)(2,1)S(1)} %get-tuple-element.23.hi, bf16[384,2048]{1,0:T(8,128)(2,1)S(1)} %get-tuple-element.24.lo, bf16[2048,128]{1,0:T(8,128)(2,1)} %bitcast.1.basis.mine), custom_call_target="tpu_custom_call" | custom-call | flops 402653184 | bytes 3670016 | tf_op jit(solution)/shard_map/project_mine/pallas_call | solution.py:227
  49.4 0.0 collective-permute-done.basis
  49.4 1.1 project_other.1
  50.5 0.1 reshape.37
  50.6 22.2 %all_to_all.20 = f32[64,4,384]{2,1,0:T(4,128)S(1)} all-to-all(f32[64,4,384]{2,1,0:T(4,128)S(1)} %reshape.37), channel_id=1, replica_groups=mesh['fs_0'=8,'fs_1'=8,'tp_0'=4,'tp_1'=2] {'fs_0','fs_1'}, dimensions={0} | all-to-all | bytes 786432 | tf_op jit(solution)/shard_map/all_to_all | solution.py:246
  72.8 0.1 reduce_sum.9.own_low
  73.0 0.1 broadcast_in_dim.3
  73.0 19.1 %all_to_all.21 = bf16[64,4,384]{2,1,0:T(4,128)(2,1)S(1)} all-to-all(bf16[64,4,384]{2,1,0:T(4,128)(2,1)S(1)} %broadcast_in_dim.3), channel_id=1, replica_groups=mesh['fs_0'=8,'fs_1'=8,'tp_0'=4,'tp_1'=2] {'fs_0','fs_1'}, dimensions={0} | all-to-all | bytes 393216 | tf_op jit(solution)/shard_map/all_to_all | solution.py:193
  92.1 0.1 reshape.38.low
  92.2 0.8 squares.1
  93.0 4.3 %all-to-all-start.3 = ((f32[8,8,128]{2,1,0:T(8,128)}), f32[8,8,128]{2,1,0:T(8,128)S(1)}, u32[]{:S(2)}, u32[]{:S(2)}) async-start(f32[8,8,128]{2,1,0:T(8,128)} %squares.1), calls=%async_computation.3 | async-start | bytes 65536 | tf_op jit(solution)/shard_map/all_to_all | solution.py:258
  97.3 1.3 %prep.1 = (bf16[2048,256]{1,0:T(8,128)(2,1)S(1)}, bf16[32,256]{1,0:T(8,128)(2,1)S(1)}, f32[32,384]{1,0:T(8,128)S(1)}, f32[4,384]{1,0:T(4,128)S(1)}, f32[4,384]{1,0:T(4,128)S(1)}) custom-call(s32[1]{0:T(128)} %bitcast.core, bf16[2048,128]{1,0:T(8,128)(2,1)} %bitcast.1.basis.mine, bf16[2048,128]{1,0:T(8,128)(2,1)} %get-tuple-element.27.other, ...), custom_call_target="tpu_custom_call" | custom-call | flops 201326592 | bytes 2097152 | tf_op jit(solution)/shard_map/prep/pallas_call | solution.py:261
  98.6 4.1 %all-to-all-done.3.squares = f32[8,8,128]{2,1,0:T(8,128)S(1)} async-done(((f32[8,8,128]{2,1,0:T(8,128)}), f32[8,8,128]{2,1,0:T(8,128)S(1)}, u32[]{:S(2)}, u32[]{:S(2)}) %all-to-all-start.3) | async-done | bytes 32800 | tf_op jit(solution)/shard_map/all_to_all | solution.py:258
  102.8 4.5 %all-gather.2.cloned.1.call-done = bf16[2560,384]{1,0:T(8,128)(2,1)} async-done(((bf16[40,384]{1,0:T(8,128)(2,1)}), bf16[2560,384]{1,0:T(8,128)(2,1)}) %all-gather.2.cloned.1.call-update) | async-done | bytes 1966096 | tf_op jit(solution)/shard_map/all_gather | solution.py:217
  107.3 3.8 %update.1 = (f32[32,128]{1,0:T(8,128)}, f32[32,256]{1,0:T(8,128)}, f32[32,128]{1,0:T(8,128)}, f32[32,256]{1,0:T(8,128)}, bf16[2048,128]{1,0:T(8,128)(2,1)}, /*in...) custom-call(f32[8,8,128]{2,1,0:T(8,128)S(1)} %all-to-all-done.3.squares, ...), custom_call_target="tpu_custom_call" | custom-call | tf_op jit(solution)/shard_map/update/pallas_call | solution.py:288
  (1 shorter events, 0.0 us)
Async XLA Ops:
  7.2 100.1 %all-gather.2.cloned.1.call-start = ((), (), s32[]{:S(2)}) async-start(), calls=%async_computation.4 | async-start | bytes 1996800 | tf_op jit(solution)/shard_map/all_gather | solution.py:217
  8.9 36.5 %all-to-all-start = ((bf16[64,32,128]{2,1,0:T(8,128)(2,1)}), bf16[64,32,128]{2,1,0:T(8,128)(2,1)}, u32[]{:S(2)}, u32[]{:S(2)}) async-start(bf16[64,32,128]{2,1,0:T(8,128)(2,1)} %get-tuple-element.22), calls=%async_computation | async-start | bytes 1048576 | tf_op jit(solution)/shard_map/all_to_all | solution.py:218
  45.4 4.0 %collective-permute-start = (bf16[2048,128]{1,0:T(8,128)(2,1)}, bf16[2048,128]{1,0:T(8,128)(2,1)S(1)}, u32[]{:S(2)}, u32[]{:S(2)}) collective-permute-start(bf16[2048,128]{1,0:T(8,128)(2,1)} %bitcast.1.basis.mine), channel_id=1, source_target_pairs={{0,1},{1,0},{2,3},{3,2},{4,5},{5,4},{6,7},{7,6},{8,9},{9,8},{10,11... | collective-permute-start | bytes 1572872 | tf_op jit(solution)/shard_map/ppermute | solution.py:225
  93.0 9.7 %all-to-all-start.3 = ((f32[8,8,128]{2,1,0:T(8,128)}), f32[8,8,128]{2,1,0:T(8,128)S(1)}, u32[]{:S(2)}, u32[]{:S(2)}) async-start(f32[8,8,128]{2,1,0:T(8,128)} %squares.1), calls=%async_computation.3 | async-start | bytes 65536 | tf_op jit(solution)/shard_map/all_to_all | solution.py:258
Sparse Core Ops, SparseCore 0:
  11.6 95.6 all-gather.1

commit v7 on v6

--- a/solution.py
+++ b/solution.py
@@ -70,8 +70,8 @@
     b = basis[...]
     at = pl.multiple_of(core[0] * half, half)
     other = pl.multiple_of((1 - core[0]) * half, half)
-    out[pl.ds(at, half), :] = mine[...]
-    out[pl.ds(other, half), :] = (dot(hi[...], b) + dot(lo[...], b)).T
+    out[pl.ds(at, half), :] = mine[...].astype(bf16)
+    out[pl.ds(other, half), :] = (dot(hi[...], b) + dot(lo[...], b)).T.astype(bf16)
     keep.wait()
 
 
@@ -235,7 +235,7 @@
     )(hi, lo, basis_mine)
     parts, basis_other = pl.pallas_call(
         project_both_kernel,
-        out_shape=(shape((R, cols), f32), pltpu.HBM((d, half), bf16)),
+        out_shape=(shape((R, cols), bf16), pltpu.HBM((d, half), bf16)),
         in_specs=[SMEM] + [VMEM] * 4,
         out_specs=(VMEM, HBM),
         scratch_shapes=[pltpu.SemaphoreType.DMA],
@@ -244,7 +244,7 @@
         name="project_other",
     )(core, hi, lo, basis_other, low_mine)
     tiles = lax.all_to_all(parts.reshape(n_fs, own, cols), FS, 0, 0, tiled=True)
-    own_low = jnp.sum(tiles, axis=0)
+    own_low = jnp.sum(tiles.astype(f32), axis=0)
 
     all_low = to_everyone(own_low.astype(bf16), FS).reshape(R, cols)
     local = pl.pallas_call(

time: 118 us -> 117 us (level)
  the two profiles are of different devices: /device:TPU:8 before, /device:TPU:2 now
where the time goes in v7:
time: 117 us; the launch traced here: 116 us
  blocking collectives  38 us (32%)
  waiting for transfers between devices  25.1 us (21%)
  starting transfers between devices  23.5 us (20%)
  between operations  14.1 us (12%)
  Pallas kernels  10.7 us (9%)
  matrix products  4.28 us (4%)
    all_to_all x1, blocking collectives, on_device(): tiles = lax.all_to_all(parts.reshape(n_fs, own, cols), FS, 0, 0, tiled=True)  19.3 us
    all_to_all x1, blocking collectives, to_everyone(): return lax.all_to_all(copies, axis, split_axis=0, concat_axis=0, tiled=True)  18.7 us
    all_to_all x1, starting transfers between devices, on_device(): basis_mine = lax.all_to_all(copies, FS, 0, 0, tiled=True).reshape(d, half)  16.9 us
    all_to_all x1, waiting for transfers between devices, on_device(): basis_mine = lax.all_to_all(copies, FS, 0, 0, tiled=True).reshape(d, half)  15.5 us
    all_gather x1, waiting for transfers between devices, on_device(): lax.all_gather(pack, FS, axis=0, tiled=True).reshape(n_fs, per, cols)  6.9 us
    all_to_all x1, starting transfers between devices, on_device(): squares = lax.all_to_all(local, TP, 0, 0, tiled=True)  4.7 us
    dot_general x1, matrix products, on_device(): lax.dot_general(cot, normed, (((0,), (0,)), ((), ())), preferred_element_...  4.28 us
    pallas_call x1, Pallas kernels, on_device(): pl.pallas_call(final_kernel, out_shape=outs[:4] + (shape((d, kc), bf16),...  3.81 us
  transfers between devices with their start and end apart: 4, of which 3 were waited for; matrix products, arithmetic and copies ran while one was open for 4% of the time, Pallas kernels for 5%

profile of v7, /device:TPU:2, one launch (start us, length us, event | category | flops | bytes accessed | tf_op | source)
XLA Modules:
  0.0 116.0 jit_solution(2971890587778056633)
XLA Ops:
  7.2 0.0 all-gather.2.cloned.1.call-start
  7.2 1.7 %pack.1 = (bf16[40,384]{1,0:T(8,128)(2,1)}, bf16[64,32,128]{2,1,0:T(8,128)(2,1)}) custom-call(s32[1]{0:T(128)} %bitcast.core, f32[32,128]{1,0:T(8,128)} %mk.3, f32[32,256]{1,0:T(8,128)} %mv.3, f32[4,128]{1,0:T(4,128)} %fk.3, f32[4,256]{1,0:T(4,128)} %fv.3, f32[4,128]{1,0:T(4,128)} %sk.3, f32[4,256]{1,0:T(4,128)} %sv.3, bf16[32,256]{1,0:T(8,128)(2,1)} %basis.3), custom_call_target="tpu_custom_call" | custom-call | tf_op jit(solution)/shard_map/pack/pallas_call | solution.py:209
  8.9 0.0 all-gather.2.cloned.1.call-update
  8.9 16.9 %all-to-all-start = ((bf16[64,32,128]{2,1,0:T(8,128)(2,1)}), bf16[64,32,128]{2,1,0:T(8,128)(2,1)}, u32[]{:S(2)}, u32[]{:S(2)}) async-start(bf16[64,32,128]{2,1,0:T(8,128)(2,1)} %get-tuple-element.22), calls=%async_computation | async-start | bytes 1048576 | tf_op jit(solution)/shard_map/all_to_all | solution.py:218
  25.8 4.3 %subtract_convert_fusion = (bf16[384,2048]{1,0:T(8,128)(2,1)S(1)}, bf16[384,2048]{1,0:T(8,128)(2,1)S(1)}) fusion(bf16[1024,2048]{1,0:T(8,128)(2,1)} %param.10, bf16[1024,256]{1,0:T(8,128)(2,1)} %param.12, bf16[1024,128]{1,0:T(8,128)(2,1)} %param.11), kind=kOutput, calls=%fused_computation | convolution fusion | flops 1615331328 | bytes 8126464 | tf_op jit(solution)/shard_map/dot_general | solution.py:221
  30.1 15.5 %all-to-all-done = bf16[64,32,128]{2,1,0:T(8,128)(2,1)} async-done(((bf16[64,32,128]{2,1,0:T(8,128)(2,1)}), bf16[64,32,128]{2,1,0:T(8,128)(2,1)}, u32[]{:S(2)}, u32[]{:S(2)}) %all-to-all-start) | async-done | bytes 524320 | tf_op jit(solution)/shard_map/all_to_all | solution.py:218
  45.5 1.9 %collective-permute-start = (bf16[2048,128]{1,0:T(8,128)(2,1)}, bf16[2048,128]{1,0:T(8,128)(2,1)S(1)}, u32[]{:S(2)}, u32[]{:S(2)}) collective-permute-start(bf16[2048,128]{1,0:T(8,128)(2,1)} %bitcast.1.basis.mine), channel_id=1, source_target_pairs={{0,1},{1,0},{2,3},{3,2},{4,5},{5,4},{6,7},{7,6},{8,9},{9,8},{10,11... | collective-permute-start | bytes 1572872 | tf_op jit(solution)/shard_map/ppermute | solution.py:225
  47.4 2.1 %project_mine.1.mine = f32[128,384]{1,0:T(8,128)S(1)} custom-call(bf16[384,2048]{1,0:T(8,128)(2,1)S(1)} %get-tuple-element.23.hi, bf16[384,2048]{1,0:T(8,128)(2,1)S(1)} %get-tuple-element.24.lo, bf16[2048,128]{1,0:T(8,128)(2,1)} %bitcast.1.basis.mine), custom_call_target="tpu_custom_call" | custom-call | flops 402653184 | bytes 3670016 | tf_op jit(solution)/shard_map/project_mine/pallas_call | solution.py:227
  49.5 0.0 collective-permute-done.basis
  49.5 1.1 project_other.1
  50.6 0.1 reshape.37
  50.7 19.3 %all_to_all.20 = bf16[64,4,384]{2,1,0:T(4,128)(2,1)S(1)} all-to-all(bf16[64,4,384]{2,1,0:T(4,128)(2,1)S(1)} %reshape.37), channel_id=1, replica_groups=mesh['fs_0'=8,'fs_1'=8,'tp_0'=4,'tp_1'=2] {'fs_0','fs_1'}, dimensions={0} | all-to-all | bytes 393216 | tf_op jit(solution)/shard_map/all_to_all | solution.py:246
  69.9 0.1 convert_reduce_fusion.own_low
  70.1 0.1 broadcast_in_dim.3
  70.1 18.7 %all_to_all.21 = bf16[64,4,384]{2,1,0:T(4,128)(2,1)S(1)} all-to-all(bf16[64,4,384]{2,1,0:T(4,128)(2,1)S(1)} %broadcast_in_dim.3), channel_id=1, replica_groups=mesh['fs_0'=8,'fs_1'=8,'tp_0'=4,'tp_1'=2] {'fs_0','fs_1'}, dimensions={0} | all-to-all | bytes 393216 | tf_op jit(solution)/shard_map/all_to_all | solution.py:193
  88.8 0.1 reshape.38.low
  88.9 0.8 squares.1
  89.7 4.7 %all-to-all-start.3 = ((f32[8,8,128]{2,1,0:T(8,128)}), f32[8,8,128]{2,1,0:T(8,128)S(1)}, u32[]{:S(2)}, u32[]{:S(2)}) async-start(f32[8,8,128]{2,1,0:T(8,128)} %squares.1), calls=%async_computation.3 | async-start | bytes 65536 | tf_op jit(solution)/shard_map/all_to_all | solution.py:258
  94.4 1.3 %prep.1 = (bf16[2048,256]{1,0:T(8,128)(2,1)S(1)}, bf16[32,256]{1,0:T(8,128)(2,1)S(1)}, f32[32,384]{1,0:T(8,128)S(1)}, f32[4,384]{1,0:T(4,128)S(1)}, f32[4,384]{1,0:T(4,128)S(1)}) custom-call(s32[1]{0:T(128)} %bitcast.core, bf16[2048,128]{1,0:T(8,128)(2,1)} %bitcast.1.basis.mine, bf16[2048,128]{1,0:T(8,128)(2,1)} %get-tuple-element.27.other, ...), custom_call_target="tpu_custom_call" | custom-call | flops 201326592 | bytes 2097152 | tf_op jit(solution)/shard_map/prep/pallas_call | solution.py:261
  95.7 2.7 %all-to-all-done.3.squares = f32[8,8,128]{2,1,0:T(8,128)S(1)} async-done(((f32[8,8,128]{2,1,0:T(8,128)}), f32[8,8,128]{2,1,0:T(8,128)S(1)}, u32[]{:S(2)}, u32[]{:S(2)}) %all-to-all-start.3) | async-done | bytes 32800 | tf_op jit(solution)/shard_map/all_to_all | solution.py:258
  98.4 6.9 %all-gather.2.cloned.1.call-done = bf16[2560,384]{1,0:T(8,128)(2,1)} async-done(((bf16[40,384]{1,0:T(8,128)(2,1)}), bf16[2560,384]{1,0:T(8,128)(2,1)}) %all-gather.2.cloned.1.call-update) | async-done | bytes 1966096 | tf_op jit(solution)/shard_map/all_gather | solution.py:217
  105.3 3.8 %update.1 = (f32[32,128]{1,0:T(8,128)}, f32[32,256]{1,0:T(8,128)}, f32[32,128]{1,0:T(8,128)}, f32[32,256]{1,0:T(8,128)}, bf16[2048,128]{1,0:T(8,128)(2,1)}, /*in...) custom-call(f32[8,8,128]{2,1,0:T(8,128)S(1)} %all-to-all-done.3.squares, ...), custom_call_target="tpu_custom_call" | custom-call | tf_op jit(solution)/shard_map/update/pallas_call | solution.py:288
  (1 shorter events, 0.0 us)
Async XLA Ops:
  7.2 98.1 %all-gather.2.cloned.1.call-start = ((), (), s32[]{:S(2)}) async-start(), calls=%async_computation.4 | async-start | bytes 1996800 | tf_op jit(solution)/shard_map/all_gather | solution.py:217
  8.9 36.6 %all-to-all-start = ((bf16[64,32,128]{2,1,0:T(8,128)(2,1)}), bf16[64,32,128]{2,1,0:T(8,128)(2,1)}, u32[]{:S(2)}, u32[]{:S(2)}) async-start(bf16[64,32,128]{2,1,0:T(8,128)(2,1)} %get-tuple-element.22), calls=%async_computation | async-start | bytes 1048576 | tf_op jit(solution)/shard_map/all_to_all | solution.py:218
  45.5 4.0 %collective-permute-start = (bf16[2048,128]{1,0:T(8,128)(2,1)}, bf16[2048,128]{1,0:T(8,128)(2,1)S(1)}, u32[]{:S(2)}, u32[]{:S(2)}) collective-permute-start(bf16[2048,128]{1,0:T(8,128)(2,1)} %bitcast.1.basis.mine), channel_id=1, source_target_pairs={{0,1},{1,0},{2,3},{3,2},{4,5},{5,4},{6,7},{7,6},{8,9},{9,8},{10,11... | collective-permute-start | bytes 1572872 | tf_op jit(solution)/shard_map/ppermute | solution.py:225
  89.7 8.7 %all-to-all-start.3 = ((f32[8,8,128]{2,1,0:T(8,128)}), f32[8,8,128]{2,1,0:T(8,128)S(1)}, u32[]{:S(2)}, u32[]{:S(2)}) async-start(f32[8,8,128]{2,1,0:T(8,128)} %squares.1), calls=%async_computation.3 | async-start | bytes 65536 | tf_op jit(solution)/shard_map/all_to_all | solution.py:258
Sparse Core Ops, SparseCore 0:
  11.6 93.6 all-gather.1
